TPU v7x, 256 devices: a 4x2x16 block of a 4x16x16 slice. The times are simulated.
256 devices in a mesh: grp: 2 (over y), kv: 16 (over z), tp: 8 (over x, core).
Axes of the slice: x: 4, y: 2, z: 16, core: 2. Of those that a mesh axis runs over, the one named last changes fastest.
The devices are a block of a 4x16x16 slice.
Arguments:
- candidate_embeddings: bfloat16 [6144, 4096], P(('grp', 'kv'), 'tp'), parts along dimension 0, may hold values from -100 to 100
- incoming_rms_scaling: float32 [4096], replicated, may hold values from 0.1 to 1.9
- probe_projector: bfloat16 [4096, 2048], P('kv', 'tp'), may hold values from -0.09375 to 0.09375
- address_projector: bfloat16 [4096, 2048], P('kv', 'tp'), may hold values from -0.09375 to 0.09375
- content_projector: bfloat16 [4096, 2048], P('kv', 'tp'), may hold values from -0.09375 to 0.09375
- sigmoid_mask_matrix: bfloat16 [4096, 2048], P('kv', 'tp'), may hold values from -0.09375 to 0.09375
- forgetting_projector: bfloat16 [4096, 16], replicated, may hold values from -0.09375 to 0.09375
- strength_projector_matrix: bfloat16 [4096, 16], replicated, may hold values from -0.09375 to 0.09375
- channel_forgetting_rates: float32 [16], P('tp'), may hold values from -3 to 0.5
- forgetting_offset: float32 [16], P('tp'), may hold values from -1 to 1
- extra_forgetting: float32 [1536, 4, 16], P(('grp', 'kv'), None, 'tp'), parts along dimension 0, may hold values from -0.7 to 0, as said below
- outgoing_rms_scaling: float32 [128], replicated, may hold values from 0.1 to 1.9
- final_projector: bfloat16 [2048, 4096], P('tp', 'kv'), may hold values from -0.125 to 0.125
- memory_matrix: float32 [1536, 16, 128, 128], P(('grp', 'kv'), 'tp'), parts along dimension 0, may hold values from -4 to 4
- earlier_addresses: bfloat16 [1536, 4, 16, 128], P(('grp', 'kv'), None, 'tp'), parts along dimension 0, may hold values from -6 to 6
- earlier_contents: bfloat16 [1536, 4, 16, 128], P(('grp', 'kv'), None, 'tp'), parts along dimension 0, may hold values from -6 to 6
- earlier_strengths: float32 [1536, 4, 16], P(('grp', 'kv'), None, 'tp'), parts along dimension 0, may hold values from 0.1 to 0.9
- earlier_forgetting: float32 [1536, 4, 16], P(('grp', 'kv'), None, 'tp'), parts along dimension 0, may hold values from -1.5 to -0.02
- admitted_counts: int32 [1536], P(('grp', 'kv')), parts along dimension 0, may hold values from 0 to 4
Outputs:
- mixed: bfloat16 [6144, 4096], P(('grp', 'kv'), 'tp'), parts along dimension 0
- taken_state: float32 [1536, 16, 128, 128], P(('grp', 'kv'), 'tp'), parts along dimension 0
There are 2 independent parts, one for each index of `grp`. A program takes and returns all parts, laid end to end along the dimension named above; an argument that names none is the same for every part. Nothing has to cross between parts.
Inputs may be any that keep to these rules, and one draw needn't show every extreme that they name: `extra_forgetting`: mostly zero; elsewhere the logarithm of a factor between 0.5 and 0.8.
All inputs are finite; a program needn't handle non-finite values.
Results may differ from a plain program's by a relative error of at most 0.015.
Values may be sent and summed in bfloat16 or wider, within the bound.
A program may use at most 128 MiB of HBM per device.

v0:
```python
import jax
import jax.numpy as jnp
from jax import lax
from jax.sharding import PartitionSpec as P

DK = 128
P_SIZE = 4


epsilon = 1e-06


def sent_to_all(shard, axis):
    count = lax.axis_size(axis)
    return lax.all_to_all(
        jnp.broadcast_to(shard[None], (count, *shard.shape)), axis, 0, 0, tiled=True
    )


def in_order(blocks, dim):
    dims = list(blocks.shape[1:])
    dims[dim] *= blocks.shape[0]
    return jnp.moveaxis(blocks, 0, dim).reshape(dims)


def gathered_copies(shard, axis, dim):
    blocks = sent_to_all(shard, axis)
    return in_order(blocks, dim)


def side_by_side(arrays, axis, dim, along):
    ends, at = ([], 0)
    for a in arrays[:-1]:
        at += a.shape[along]
        ends.append(at)
    both = jnp.concatenate(arrays, axis=along)
    return tuple(jnp.split(lax.all_gather(both, axis, axis=dim, tiled=True), ends, axis=along))


def split_up(shard, dim, count):
    dims = shard.shape
    blocks = shard.reshape(*dims[:dim], count, dims[dim] // count, *dims[dim + 1 :])
    return jnp.moveaxis(blocks, dim, 0)


def summed_on_arrival(shard, axis, dim):
    count = lax.axis_size(axis)
    blocks = lax.all_to_all(split_up(shard, dim, count), axis, 0, 0, tiled=True)
    return jnp.sum(blocks.astype(jnp.float32), axis=0)


def unit_norm(vector):
    return vector * lax.rsqrt(jnp.sum(vector * vector, axis=-1, keepdims=True) + epsilon)


def update(carry, key_vec, value_vec, beta, log_decay):
    decayed = jnp.exp(log_decay)[..., None, None] * carry
    recalled = jnp.einsum("shde,shd->she", decayed, key_vec)
    return decayed + jnp.einsum("shd,she->shde", key_vec, beta[..., None] * (value_vec - recalled))


def stored(values):
    return lax.optimization_barrier(values.astype(jnp.bfloat16)).astype(jnp.float32)


def on_device(
    candidate_embeddings,
    incoming_rms_scaling,
    probe_projector,
    address_projector,
    content_projector,
    sigmoid_mask_matrix,
    forgetting_projector,
    strength_projector_matrix,
    channel_forgetting_rates,
    forgetting_offset,
    extra_forgetting,
    outgoing_rms_scaling,
    final_projector,
    memory_matrix,
    earlier_addresses,
    earlier_contents,
    earlier_strengths,
    earlier_forgetting,
    admitted_counts,
):
    rows, local_cols = candidate_embeddings.shape
    width = probe_projector.shape[1]
    heads = width // DK
    seqs_here = rows // P_SIZE
    head_start = lax.axis_index("tp") * heads
    whole = gathered_copies(candidate_embeddings, "tp", 1).astype(jnp.float32)
    normed = (
        whole
        * lax.rsqrt(jnp.mean(whole * whole, axis=1, keepdims=True) + epsilon)
        * incoming_rms_scaling
    ).astype(jnp.bfloat16)
    pieces = side_by_side(
        (probe_projector, address_projector, content_projector, sigmoid_mask_matrix), "kv", 0, 1
    )
    query, keyed, valued, gated = tuple(
        (jnp.dot(normed, piece, preferred_element_type=jnp.float32) for piece in pieces)
    )

    def shaped(values):
        return stored(values).reshape(seqs_here, P_SIZE, heads, DK)

    query = unit_norm(shaped(query)) * DK ** (-0.5)
    keyed = unit_norm(shaped(keyed))
    valued = shaped(valued)
    gated = shaped(gated)
    decay_cols = lax.dynamic_slice_in_dim(forgetting_projector, head_start, heads, 1)
    beta_cols = lax.dynamic_slice_in_dim(strength_projector_matrix, head_start, heads, 1)
    forgetting_argument = jnp.dot(normed, decay_cols, preferred_element_type=jnp.float32).reshape(
        seqs_here, P_SIZE, heads
    )
    beta_in = jnp.dot(normed, beta_cols, preferred_element_type=jnp.float32).reshape(
        seqs_here, P_SIZE, heads
    )
    forgetting_multiplier = (
        -jnp.exp(channel_forgetting_rates)
        * jax.nn.softplus(forgetting_argument + forgetting_offset)
        + extra_forgetting
    )
    beta = jax.nn.sigmoid(beta_in)
    carried = memory_matrix
    for proposal in range(P_SIZE):
        fresh = update(
            carried,
            unit_norm(earlier_addresses[:, proposal].astype(jnp.float32)),
            earlier_contents[:, proposal].astype(jnp.float32),
            earlier_strengths[:, proposal],
            earlier_forgetting[:, proposal],
        )
        live = (admitted_counts > proposal)[:, None, None, None]
        carried = jnp.where(live, fresh, carried)
    running = carried
    outputs = []
    for proposal in range(P_SIZE):
        running = update(
            running,
            keyed[:, proposal],
            valued[:, proposal],
            beta[:, proposal],
            forgetting_multiplier[:, proposal],
        )
        outputs.append(jnp.einsum("shde,shd->she", running, query[:, proposal]))
    attended = jnp.stack(outputs, axis=1)
    scaled = (
        attended
        * lax.rsqrt(jnp.mean(attended * attended, axis=-1, keepdims=True) + epsilon)
        * outgoing_rms_scaling
        * jax.nn.silu(gated)
    )
    flat = scaled.astype(jnp.bfloat16).reshape(rows, width)
    terms = stored(
        jnp.dot(
            flat,
            lax.all_gather(final_projector, "kv", axis=1, tiled=True),
            preferred_element_type=jnp.float32,
        )
    )
    mixed = summed_on_arrival(terms.astype(jnp.bfloat16), "tp", 1).astype(jnp.bfloat16)
    return (mixed, carried)


def solution(mesh):
    in_specs = (
        P(("grp", "kv"), "tp"),
        P(),
        P("kv", "tp"),
        P("kv", "tp"),
        P("kv", "tp"),
        P("kv", "tp"),
        P(),
        P(),
        P("tp"),
        P("tp"),
        P(("grp", "kv"), None, "tp"),
        P(),
        P("tp", "kv"),
        P(("grp", "kv"), "tp", None, None),
        P(("grp", "kv"), None, "tp", None),
        P(("grp", "kv"), None, "tp", None),
        P(("grp", "kv"), None, "tp"),
        P(("grp", "kv"), None, "tp"),
        P(("grp", "kv")),
    )
    out_specs = (P(("grp", "kv"), "tp"), P(("grp", "kv"), "tp", None, None))
    return jax.shard_map(
        on_device, mesh=mesh, in_specs=in_specs, out_specs=out_specs, check_vma=False
    )
```

profile of v0, /device:TPU:36, one launch (start us, length us, event | category | flops | bytes accessed | tf_op | source)
XLA Modules:
  0.0 238.4 jit_solution(9750153225958268776)
XLA Ops:
  7.3 2.0 pad_maximum_fusion
  9.4 2.3 broadcast_in_dim.25
  11.7 22.8 %all-to-all-start = ((bf16[8,192,512]{2,1,0:T(8,128)(2,1)}), bf16[8,192,512]{2,1,0:T(8,128)(2,1)S(1)}, u32[]{:S(2)}, u32[]{:S(2)}) async-start(bf16[8,192,512]{2,1,0:T(8,128)(2,1)} %broadcast_in_dim.25), calls=%async_computation | async-start | bytes 3145728 | tf_op jit(solution)/shard_map/all_to_all | solution.py:15
  34.5 0.8 all-gather.5.cloned.1.call-update
  35.3 0.1 copy.103
  36.0 0.3 fusion.104
  36.3 0.3 convert_multiply_fusion.8
  36.6 4.2 %fusion.18 = f32[48,2,1,128]{3,2,1,0:T(1,128)S(1)} fusion(f32[48,2,128,1]{2,3,1,0:T(1,128)S(1)} %bitcast.216, f32[48,2,128,128]{3,2,1,0:T(8,128)} %param.32, f32[48,2]{1,0:T(8,128)S(1)} %copy.106), kind=kOutput, calls=%fused_computation.25 | convolution fusion | flops 4718592 | bytes 6390144 | tf_op jit(solution)/shard_map/shde,shd->she/dot_general | solution.py:58
  40.8 0.1 fusion.119
  40.9 3.0 %fusion.16 = f32[48,2,1,128]{3,2,1,0:T(1,128)S(1)} fusion(f32[48,2,128,1]{2,3,1,0:T(1,128)S(1)} %bitcast.218, f32[48,2,128,128]{3,2,1,0:T(8,128)S(1)} %copy-done.1, f32[48,2,128]{2,1,0:T(2,128)S(1)} %fusion.119, f32[48,2,128]{2,1,0:T(2,128)S(1)} %get-tuple-element.20, f32[48,2]{1,0:T(8,128)S(1)} %copy.106, f32[48,2]{1,0:T(8,128)S(1)} %copy.105, ...), kind=kOutput, calls=%fused_computation.23 | convolution fusion | flops 11010048 | bytes 6488880 | tf_op jit(solution)/shard_map/shde,shd->she/dot_general | solution.py:58
  44.0 0.1 fusion.118
  44.1 5.9 %fusion.14 = f32[48,2,1,128]{3,2,1,0:T(1,128)S(1)} fusion(f32[48,2,128,1]{2,3,1,0:T(1,128)S(1)} %bitcast.219, f32[48,2]{1,0:T(8,128)S(1)} %copy.104, f32[48,2,128,128]{3,2,1,0:T(8,128)S(1)} %copy-done.1, f32[48,2,128]{2,1,0:T(2,128)S(1)} %fusion.118, f32[48,2,128]{2,1,0:T(2,128)S(1)} %get-tuple-element.22, f32[48,2,128]{2,1,0:T(2,128)S(1)} %fusion.119, ...), kind=kOutput, calls=%fused_computation.21 | convolution fusion | flops 17301504 | bytes 6587616 | tf_op jit(solution)/shard_map/shde,shd->she/dot_general | solution.py:58
  50.0 0.1 fusion.117
  50.1 8.5 %fusion.12 = f32[48,2,1,128]{3,2,1,0:T(1,128)S(1)} fusion(f32[48,2,128,1]{2,3,1,0:T(1,128)S(1)} %bitcast.217, f32[48,2,128]{2,1,0:T(2,128)S(1)} %fusion.117, f32[48,2,128]{2,1,0:T(2,128)S(1)} %get-tuple-element.23, f32[48,2]{1,0:T(8,128)S(1)} %copy.104, f32[48,2]{1,0:T(8,128)S(1)} %copy.103, pred[48]{0:T(512)(128)(4,1)S(1)} %get-tuple-element.41, ...), kind=kOutput, calls=%fused_computation.19 | convolution fusion | flops 23592960 | bytes 6686352 | tf_op jit(solution)/shard_map/shde,shd->she/dot_general | solution.py:58
  58.8 0.1 fusion.116
  58.9 11.2 %add_select_fusion = f32[48,2,128,128]{3,2,1,0:T(8,128)} fusion(f32[48,2,128]{2,1,0:T(2,128)S(1)} %fusion.116, f32[48,2,128]{2,1,0:T(2,128)S(1)} %get-tuple-element.21, f32[48,2,128]{2,1,0:T(2,128)S(1)} %fusion.117, f32[48,2,128]{2,1,0:T(2,128)S(1)} %get-tuple-element.23, f32[48,2]{1,0:T(8,128)S(1)} %copy.104, f32[48,2]{1,0:T(8,128)S(1)} %copy.103, ...), kind=kLoop, calls=%fused_computation.6 | loop fusion | flops 25165824 | bytes 12977856 | tf_op jit(solution)/shard_map/jit(_where)/select_n | solution.py:136
  70.1 0.4 fusion.22
  70.6 0.1 rsqrt.69
  70.7 2.2 convert_bitcast_fusion.1
  72.9 3.6 %copy.100 = f32[192,8,512]{2,1,0:T(8,128)} copy(f32[192,8,512]{2,0,1:T(8,128)S(1)} %get-tuple-element.6) | data formatting | bytes 6291456 | tf_op jit(solution)/shard_map/convert_element_type | solution.py:92
  76.4 4.1 %reshape.207 = f32[48,4,4096]{2,1,0:T(4,128)S(1)} reshape(f32[192,8,512]{2,1,0:T(8,128)} %copy.100) | data formatting | bytes 6291456 | tf_op jit(solution)/shard_map/convert_element_type | solution.py:92
  80.6 1.0 multiply_convert_fusion.1
  81.6 1.0 fusion.93
  82.7 1.8 fusion.125
  85.3 0.3 copy.152
  85.6 0.4 multiply_convert_fusion
  86.0 41.4 %all-gather.3.cloned.1.call-done = bf16[4096,1024]{1,0:T(8,128)(2,1)} async-done(((bf16[256,1024]{1,0:T(8,128)(2,1)}), bf16[4096,1024]{1,0:T(8,128)(2,1)}) %all-gather.3.cloned.1.call-update) | async-done | bytes 8388624 | tf_op jit(solution)/shard_map/all_gather | solution.py:37
  127.5 2.2 fusion.75
  129.6 0.1 reshape.222
  129.7 0.4 multiply_reduce_fusion.1
  130.1 0.1 copy.116
  130.2 2.2 fusion.69
  132.4 2.2 fusion.72
  134.5 0.1 reshape.220
  134.7 0.1 reshape.218
  134.8 0.4 multiply_reduce_fusion.2
  135.1 0.1 copy.112
  135.2 0.1 copy.113
  135.4 0.3 broadcast_multiply_fusion.1
  135.6 0.1 slice_bitcast_fusion.12
  135.8 3.9 %fusion.10 = f32[48,2,1,128]{3,2,1,0:T(1,128)S(1)} fusion(f32[48,2,128,1]{2,3,1,0:T(1,128)S(1)} %bitcast.220, f32[48,2,128,128]{3,2,1,0:T(8,128)} %add_select_fusion, f32[48,2]{1,0:T(8,128)S(1)} %copy.102), kind=kOutput, calls=%fused_computation.17 | convolution fusion | flops 4718592 | bytes 6390144 | tf_op jit(solution)/shard_map/shde,shd->she/dot_general | solution.py:58
  139.7 0.1 fusion.115
  139.8 4.6 %fusion.8 = f32[48,2,1,128]{3,2,1,0:T(1,128)S(1)} fusion(f32[48,2,128,1]{2,3,1,0:T(1,128)S(1)} %bitcast.234, f32[48,2,128,128]{3,2,1,0:T(8,128)} %add_select_fusion, f32[48,2]{1,0:T(8,128)S(1)} %copy.118, f32[48,2,128]{2,1,0:T(2,128)S(1)} %fusion.115, f32[48,2,128]{2,1,0:T(2,128)S(1)} %get-tuple-element.13, f32[48,2]{1,0:T(8,128)S(1)} %copy.102), kind=kOutput, calls=%fused_computation.15 | convolution fusion | flops 9437184 | bytes 6488832 | tf_op jit(solution)/shard_map/shde,shd->she/dot_general | solution.py:58
  144.4 0.1 fusion.113
  144.6 5.8 %fusion.6 = f32[48,2,1,128]{3,2,1,0:T(1,128)S(1)} fusion(f32[48,2,128,1]{2,3,1,0:T(1,128)S(1)} %bitcast.233, f32[48,2]{1,0:T(8,128)S(1)} %copy.120, f32[48,2,128,128]{3,2,1,0:T(8,128)S(1)} %bitcast.209, f32[48,2,128]{2,1,0:T(2,128)S(1)} %fusion.113, f32[48,2,128]{2,1,0:T(2,128)S(1)} %get-tuple-element.14, f32[48,2]{1,0:T(8,128)S(1)} %copy.118, ...), kind=kOutput, calls=%fused_computation.13 | convolution fusion | flops 14155776 | bytes 6587520 | tf_op jit(solution)/shard_map/shde,shd->she/dot_general | solution.py:58
  150.4 0.1 fusion.111
  150.5 8.3 %fusion.4 = f32[48,2,1,128]{3,2,1,0:T(1,128)S(1)} fusion(f32[48,2,128,1]{2,3,1,0:T(1,128)S(1)} %bitcast.231, f32[48,2]{1,0:T(8,128)S(1)} %copy.122, f32[48,2,128]{2,1,0:T(2,128)S(1)} %fusion.111, f32[48,2,128]{2,1,0:T(2,128)S(1)} %get-tuple-element.15, f32[48,2]{1,0:T(8,128)S(1)} %copy.120, f32[48,2,128,128]{3,2,1,0:T(8,128)S(1)} %bitcast.209, ...), kind=kOutput, calls=%fused_computation.11 | convolution fusion | flops 18874368 | bytes 6686208 | tf_op jit(solution)/shard_map/shde,shd->she/dot_general | solution.py:58
  158.9 2.2 fusion.78
  161.1 0.1 copy.117
  161.2 0.1 fusion.109
  161.3 0.3 multiply_multiply_fusion
  161.7 4.0 %fusion.20 = f32[48,2,1,128]{3,2,1,0:T(1,128)S(1)} fusion(f32[48,2,128,1]{2,3,1,0:T(1,128)S(1)} %bitcast.237, f32[48,2,128,128]{3,2,1,0:T(8,128)} %add_select_fusion, f32[48,2,128]{2,1,0:T(2,128)S(1)} %fusion.115, f32[48,2,128]{2,1,0:T(2,128)S(1)} %get-tuple-element.13, f32[48,2]{1,0:T(8,128)S(1)} %copy.102), kind=kOutput, calls=%fused_computation.31 | convolution fusion | flops 7864320 | bytes 6488448 | tf_op jit(solution)/shard_map/shde,shd->she/dot_general | solution.py:147
  165.7 6.3 %fusion.137 = f32[48,2,1,128]{3,2,1,0:T(1,128)S(1)} fusion(f32[48,2,128,1]{2,3,1,0:T(1,128)S(1)} %bitcast.236, f32[48,2,128,128]{3,2,1,0:T(8,128)} %add_select_fusion, f32[48,2,128]{2,1,0:T(2,128)S(1)} %fusion.113, f32[48,2,128]{2,1,0:T(2,128)S(1)} %get-tuple-element.14, f32[48,2]{1,0:T(8,128)S(1)} %copy.118, f32[48,2,128]{2,1,0:T(2,128)S(1)} %fusion.115, ...), kind=kOutput, calls=%fused_computation.190 | convolution fusion | flops 12582912 | bytes 6587136 | tf_op jit(solution)/shard_map/shde,shd->she/dot_general | solution.py:147
  172.0 8.4 %fusion.21 = f32[48,2,1,128]{3,2,1,0:T(1,128)S(1)} fusion(f32[48,2,128,1]{2,3,1,0:T(1,128)S(1)} %bitcast.235, f32[48,2,128]{2,1,0:T(2,128)S(1)} %fusion.111, f32[48,2,128]{2,1,0:T(2,128)S(1)} %get-tuple-element.15, f32[48,2]{1,0:T(8,128)S(1)} %copy.120, f32[48,2,128,128]{3,2,1,0:T(8,128)S(1)} %bitcast.211, f32[48,2,128]{2,1,0:T(2,128)S(1)} %fusion.113, ...), kind=kOutput, calls=%fused_computation.32 | convolution fusion | flops 17301504 | bytes 6685824 | tf_op jit(solution)/shard_map/shde,shd->she/dot_general | solution.py:147
  180.5 11.4 %fusion = f32[48,2,1,128]{3,2,1,0:T(1,128)S(1)} fusion(f32[48,2,128,1]{2,3,1,0:T(1,128)S(1)} %bitcast.232, f32[48,2,128]{2,1,0:T(2,128)S(1)} %fusion.109, f32[48,2,128]{2,1,0:T(2,128)S(1)} %get-tuple-element.12, f32[48,2]{1,0:T(8,128)S(1)} %copy.122, f32[48,2,128]{2,1,0:T(2,128)S(1)} %fusion.111, f32[48,2,128]{2,1,0:T(2,128)S(1)} %get-tuple-element.15, ...), kind=kOutput, calls=%fused_computation | convolution fusion | flops 22020096 | bytes 6784512 | tf_op jit(solution)/shard_map/shde,shd->she/dot_general | solution.py:147
  191.9 0.4 multiply_reduce_fusion
  192.2 0.1 copy.124
  192.3 0.1 copy.125
  192.5 0.3 broadcast_multiply_fusion
  192.7 12.3 %all-gather.5.cloned.1.call-done = bf16[256,4096]{1,0:T(8,128)(2,1)} async-done(((bf16[256,256]{1,0:T(8,128)(2,1)}), bf16[256,4096]{1,0:T(8,128)(2,1)}) %all-gather.5.cloned.1.call-update) | async-done | bytes 2097168 | tf_op jit(solution)/shard_map/all_gather | solution.py:159
  205.1 2.2 convolution_convert_fusion
  207.2 0.1 copy.175
  207.4 23.3 %all_to_all.10 = bf16[8,192,512]{2,1,0:T(8,128)(2,1)S(1)} all-to-all(bf16[8,192,512]{2,1,0:T(8,128)(2,1)S(1)} %bitcast.214), channel_id=1, replica_groups=mesh['grp'=2,'kv'=16,'tp'=8] {'tp'}, dimensions={0} | all-to-all | bytes 3145728 | tf_op jit(solution)/shard_map/all_to_all | solution.py:48
  230.6 0.9 reduce_sum.92
  (69 shorter events, 1.7 us)
Async XLA Ops:
  7.2 74.4 %copy-start = (bf16[4096,16]{0,1:T(8,128)(2,1)S(1)}, bf16[4096,16]{0,1:T(8,128)(2,1)}, u32[]{:S(2)}) copy-start(bf16[4096,16]{0,1:T(8,128)(2,1)} %param.26) | copy-start | bytes 393220
  7.2 28.0 %copy-start.10 = (f32[128]{0:T(128)S(1)}, f32[128]{0:T(128)}, u32[]{:S(2)}) copy-start(f32[128]{0:T(128)} %param.30) | copy-start | bytes 1540
  7.2 28.1 %copy-start.8 = (s32[48]{0:T(128)S(1)}, s32[48]{0:T(128)}, u32[]{:S(2)}) copy-start(s32[48]{0:T(128)} %param.37) | copy-start | bytes 580
  7.2 28.1 %copy-start.6 = (f32[48,4,2]{0,2,1:T(2,128)S(1)}, f32[48,4,2]{0,2,1:T(2,128)}, u32[]{:S(2)}) copy-start(f32[48,4,2]{0,2,1:T(2,128)} %param.35) | copy-start | bytes 4612
  7.2 28.1 %copy-start.7 = (f32[48,4,2]{0,2,1:T(2,128)S(1)}, f32[48,4,2]{0,2,1:T(2,128)}, u32[]{:S(2)}) copy-start(f32[48,4,2]{0,2,1:T(2,128)} %param.36) | copy-start | bytes 4612
  7.2 28.7 %copy-start.3 = (bf16[48,4,2,128]{3,2,1,0:T(2,128)(2,1)S(1)}, bf16[48,4,2,128]{3,2,1,0:T(2,128)(2,1)}, u32[]{:S(2)}) copy-start(bf16[48,4,2,128]{3,2,1,0:T(2,128)(2,1)} %param.33) | copy-start | bytes 294916
  7.2 120.2 %all-gather.3.cloned.1.call-start = ((), (), s32[]{:S(2)}) async-start(), calls=%async_computation.2 | async-start | bytes 8912896 | tf_op jit(solution)/shard_map/all_gather | solution.py:37
  9.4 31.4 %copy-start.4 = (bf16[48,4,2,128]{3,2,1,0:T(2,128)(2,1)S(1)}, bf16[48,4,2,128]{3,2,1,0:T(2,128)(2,1)}, u32[]{:S(2)}) copy-start(bf16[48,4,2,128]{3,2,1,0:T(2,128)(2,1)} %param.34) | copy-start | bytes 294916
  11.7 58.5 %all-to-all-start = ((bf16[8,192,512]{2,1,0:T(8,128)(2,1)}), bf16[8,192,512]{2,1,0:T(8,128)(2,1)S(1)}, u32[]{:S(2)}, u32[]{:S(2)}) async-start(bf16[8,192,512]{2,1,0:T(8,128)(2,1)} %broadcast_in_dim.25), calls=%async_computation | async-start | bytes 3145728 | tf_op jit(solution)/shard_map/all_to_all | solution.py:15
  34.5 170.6 %all-gather.5.cloned.1.call-start = ((), (), s32[]{:S(2)}) async-start(), calls=%async_computation.3 | async-start | bytes 2228224 | tf_op jit(solution)/shard_map/all_gather | solution.py:159
  36.0 5.0 %copy-start.1 = (f32[48,2,128,128]{3,2,1,0:T(8,128)S(1)}, f32[48,2,128,128]{3,2,1,0:T(8,128)}, u32[]{:S(2)}) copy-start(f32[48,2,128,128]{3,2,1,0:T(8,128)} %param.32) | copy-start | bytes 18874372
  50.1 8.5 %copy-start.11 = (f32[2]{0:T(128)S(1)}, f32[2]{0:T(128)}, u32[]{:S(2)}) copy-start(f32[2]{0:T(128)} %param.27) | copy-start | bytes 28
  72.9 7.7 %copy-start.5 = (f32[4096]{0:T(1024)S(1)}, f32[4096]{0:T(1024)}, u32[]{:S(2)}) copy-start(f32[4096]{0:T(1024)} %param.20) | copy-start | bytes 49156
  76.4 6.2 %copy-start.9 = (f32[48,4,2]{0,2,1:T(2,128)S(1)}, f32[48,4,2]{0,2,1:T(2,128)}, u32[]{:S(2)}) copy-start(f32[48,4,2]{0,2,1:T(2,128)} %param.29) | copy-start | bytes 4612
  76.4 6.2 %copy-start.12 = (f32[2]{0:T(128)S(1)}, f32[2]{0:T(128)}, u32[]{:S(2)}) copy-start(f32[2]{0:T(128)} %param.28) | copy-start | bytes 28
  81.6 3.6 %copy-start.2 = (f32[8,24,8,512]{3,2,1,0:T(8,128)S(1)}, f32[8,24,8,512]{3,2,1,0:T(8,128)}, u32[]{:S(2)}) copy-start(f32[8,24,8,512]{3,2,1,0:T(8,128)} %get-tuple-element.7) | copy-start | bytes 9437188
  135.8 8.8 %slice-start = ((s8[6291456]{0:T(1024)(128)(4,1)}), s8[2097152]{0:T(1024)(128)(4,1)S(1)}, s32[]{:S(2)}) async-start(s8[6291456]{0:T(1024)(128)(4,1)} %bitcast.208), calls=%async_computation.4 | async-start | bytes 4194304
  139.8 4.8 %slice-start.1 = ((s8[6291456]{0:T(1024)(128)(4,1)}), s8[4194304]{0:T(1024)(128)(4,1)S(1)}, s32[]{:S(2)}) async-start(s8[6291456]{0:T(1024)(128)(4,1)} %bitcast.208), calls=%async_computation.5 | async-start | bytes 8388608
  165.7 6.4 %slice-start.2 = ((s8[6291456]{0:T(1024)(128)(4,1)}), s8[4194304]{0:T(1024)(128)(4,1)S(1)}, s32[]{:S(2)}) async-start(s8[6291456]{0:T(1024)(128)(4,1)} %bitcast.210), calls=%async_computation.6 | async-start | bytes 8388608
  165.7 6.4 %slice-start.3 = ((s8[6291456]{0:T(1024)(128)(4,1)}), s8[2097152]{0:T(1024)(128)(4,1)S(1)}, s32[]{:S(2)}) async-start(s8[6291456]{0:T(1024)(128)(4,1)} %bitcast.210), calls=%async_computation.7 | async-start | bytes 4194304
Sparse Core Ops, SparseCore 0:
  9.9 117.5 all-gather.2
  129.2 75.8 all-gather.4
where the time goes:
time: 242 us; the launch traced here: 238 us
  matrix products  88.2 us (36%)
  waiting for transfers between devices  54.5 us (23%)
  blocking collectives  23.3 us (10%)
  starting transfers between devices  22.8 us (9%)
  other arithmetic  21.7 us (9%)
  between operations  14.6 us (6%)
  local copies, waits for them, and re-layouts  13.3 us (5%)
    dot_general x8, matrix products, update(): recalled = jnp.einsum('shde,shd->she', decayed, key_vec)  44.3 us
    all_gather x1, waiting for transfers between devices, side_by_side(): lax.all_gather(both, axis, axis=dim, tiled=True)  41.4 us
    dot_general x4, matrix products, on_device(): outputs.append(jnp.einsum('shde,shd->she', running, query[:, proposal]))  30.2 us
    all_to_all x1, blocking collectives, summed_on_arrival(): blocks = lax.all_to_all(split_up(shard, dim, count), axis, 0, 0, tiled=True)  23.3 us
    all_to_all x1, starting transfers between devices, sent_to_all(): lax.all_to_all(jnp.broadcast_to(shard[None], (count, *shard.shape)), axis...  22.8 us
    all_gather x1, waiting for transfers between devices, on_device(): lax.all_gather(final_projector, 'kv', axis=1, tiled=True)  12.3 us
    select_n x1, other arithmetic, on_device(): carried = jnp.where(live, fresh, carried)  11.2 us
    dot_general x4, matrix products, on_device(): jnp.dot(normed, piece, preferred_element_type=jnp.float32)  8.69 us
  transfers between devices with their start and end apart: 3, of which 2 were waited for; matrix products, arithmetic and copies ran while one was open for 49% of the time, Pallas kernels for 0%

commit v1 on v0

v1 whole, which is shorter than its diff:
```python
import functools

import jax
import jax.numpy as jnp
from jax import lax
from jax.experimental import pallas as pl
from jax.experimental.pallas import tpu as pltpu
from jax.sharding import PartitionSpec as P

DK = 128
P_SIZE = 4
W_SUB = 2
F_SUB = 4

epsilon = 1e-06
MESH = pl.DeviceIdType.MESH
BF = jnp.bfloat16
F32 = jnp.float32


def unit_norm(vector):
    return vector * lax.rsqrt(jnp.sum(vector * vector, axis=-1, keepdims=True) + epsilon)


def mm(a, b):
    return jnp.dot(a.astype(BF), b.astype(BF), preferred_element_type=F32)


def mm_t(a, b):
    return lax.dot_general(
        a.astype(BF), b.astype(BF), (((1,), (1,)), ((), ())), preferred_element_type=F32
    )


def group_masks(count):
    row = lax.broadcasted_iota(jnp.int32, (count, count), 0)
    col = lax.broadcasted_iota(jnp.int32, (count, count), 1)
    same = (row // P_SIZE) == (col // P_SIZE)
    return row == col, same, same & (col <= row), same & (col < row)


def decay_terms(log_decay, masks):
    eye, same, upto, _ = masks
    along = jnp.sum(jnp.where(eye, log_decay, 0.0), axis=0, keepdims=True)
    summed = jnp.sum(jnp.where(upto, along, 0.0), axis=1, keepdims=True)
    total = jnp.sum(jnp.where(same, along, 0.0), axis=1, keepdims=True)
    summed_along = jnp.sum(jnp.where(eye, summed, 0.0), axis=0, keepdims=True)
    between = jnp.exp(jnp.where(upto, summed - summed_along, -1e30))
    return summed, total, between


def corrections(keys, wanted, beta, between, masks):
    lower = jnp.where(masks[3], beta * between * mm_t(keys, keys), 0.0)
    both = wanted + mm(lower, mm(lower, wanted))
    return both - mm(lower, both)


def taken_kernel(keys_ref, values_ref, scalars_ref, state_ref, out_ref):
    seqs, heads = state_ref.shape[:2]
    rows = keys_ref.shape[0]
    masks = group_masks(rows)
    group = lax.broadcasted_iota(jnp.int32, (rows, DK), 0) // P_SIZE
    for h in range(heads):
        cols = slice(h * DK, (h + 1) * DK)
        beta = scalars_ref[:, h : h + 1]
        summed, total, between = decay_terms(scalars_ref[:, heads + h : heads + h + 1], masks)
        keys = unit_norm(keys_ref[:, cols].astype(F32))
        recalled = jnp.zeros((rows, DK), F32)
        for s in range(seqs):
            recalled = jnp.where(group == s, mm(keys, state_ref[s, h]), recalled)
        wanted = beta * (values_ref[:, cols].astype(F32) - jnp.exp(summed) * recalled)
        fixes = jnp.exp(total - summed) * corrections(keys, wanted, beta, between, masks)
        spread = jnp.concatenate([jnp.where(group == s, fixes, 0.0) for s in range(seqs)], axis=1)
        added = lax.dot_general(
            keys.astype(BF),
            spread.astype(BF),
            (((0,), (0,)), ((), ())),
            preferred_element_type=F32,
        )
        kept = jnp.exp(total)
        for s in range(seqs):
            scale = kept[s * P_SIZE : s * P_SIZE + 1, :]
            out_ref[s, h] = scale * state_ref[s, h] + added[:, s * DK : (s + 1) * DK]


def taken_state_of(keys, values, scalars, state, block=8):
    seqs, heads = state.shape[:2]
    rows = block * P_SIZE
    width = keys.shape[1]
    return pl.pallas_call(
        taken_kernel,
        grid=(seqs // block,),
        in_specs=[
            pl.BlockSpec((rows, width), lambda i: (i, 0)),
            pl.BlockSpec((rows, width), lambda i: (i, 0)),
            pl.BlockSpec((rows, scalars.shape[1]), lambda i: (i, 0)),
            pl.BlockSpec((block, heads, DK, DK), lambda i: (i, 0, 0, 0)),
        ],
        out_specs=pl.BlockSpec((block, heads, DK, DK), lambda i: (i, 0, 0, 0)),
        out_shape=jax.ShapeDtypeStruct(state.shape, F32),
        cost_estimate=pl.CostEstimate(
            flops=state.size * 32, bytes_accessed=state.size * 8, transcendentals=0
        ),
    )(keys, values, scalars, state)


def mix_kernel(
    n_z,
    n_x,
    cand_ref,
    gain_ref,
    wq_ref,
    wk_ref,
    wv_ref,
    wg_ref,
    fb_ref,
    rates_ref,
    offset_ref,
    extra_ref,
    out_gain_ref,
    proj_ref,
    taken_ref,
    out_ref,
    a_buf,
    n_buf,
    w_buf,
    f_buf,
    t_buf,
    acc,
    c_send,
    c_buf,
    kn_buf,
    qn_buf,
    kt_buf,
    qt_buf,
    scal_buf,
    flat,
    p_buf,
    s_buf,
    r_buf,
    x_send,
    x_buf,
    own,
    local_sem,
    wload_sem,
    y_send,
    y_recv,
    ax_send,
    ax_recv,
    as_send,
    as_recv,
    w_send,
    w_recv,
    f_send,
    f_recv,
    c_ssem,
    c_rsem,
    rs_send,
    rs_recv,
    rx_send,
    rx_recv,
):
    rows, mine = cand_ref.shape
    depth = proj_ref.shape[1]
    heads = proj_ref.shape[0] // DK
    half = n_z // 2
    tp = lax.axis_index("tp")
    me = lax.axis_index("kv")
    grp = lax.axis_index("grp")
    x = tp // 2
    core = tp % 2
    side = grp % 2
    z_dev = ({"kv": (me + 1) % n_z}, {"kv": (me + n_z - 1) % n_z})
    y_dev = {"grp": grp + 1 - 2 * side}
    x_dev = [{"tp": ((x + d) % n_x) * 2 + core} for d in range(n_x)]
    sib_dev = {"tp": x * 2 + 1 - core}

    def send(src, dst, s_sem, r_sem, dev):
        return pltpu.make_async_remote_copy(
            src_ref=src,
            dst_ref=dst,
            send_sem=s_sem,
            recv_sem=r_sem,
            device_id=dev,
            device_id_type=MESH,
        )

    cand_load = pltpu.make_async_copy(
        cand_ref, a_buf.at[pl.ds(0, rows), pl.ds(pl.multiple_of(tp * mine, mine), mine)], local_sem.at[0]
    )
    cand_load.start()
    sub_rows = depth // W_SUB

    def w_loads(first, second):
        copies = []
        for i, ref in enumerate((first, second)):
            for sub in range(W_SUB):
                copies.append(
                    pltpu.make_async_copy(
                        ref.at[pl.ds(sub * sub_rows, sub_rows), :],
                        w_buf.at[me, sub, :, pl.ds(i * heads * DK, heads * DK)],
                        wload_sem.at[i, sub],
                    )
                )
        return copies

    @pl.when(side == 0)
    def _():
        for c in w_loads(wq_ref, wk_ref):
            c.start()

    @pl.when(side == 1)
    def _():
        for c in w_loads(wv_ref, wg_ref):
            c.start()

    f_rows = proj_ref.shape[0] // F_SUB
    f_loads = [
        pltpu.make_async_copy(
            proj_ref.at[pl.ds(sub * f_rows, f_rows), :], f_buf.at[me, sub], local_sem.at[2 + sub]
        )
        for sub in range(F_SUB)
    ]
    for c in f_loads:
        c.start()
    taken_load = pltpu.make_async_copy(taken_ref, t_buf, local_sem.at[1])
    taken_load.start()

    barrier = pltpu.get_barrier_semaphore()
    peers = (z_dev[0], z_dev[1], y_dev, sib_dev, *x_dev[1:])
    for dev in peers:
        pl.semaphore_signal(barrier, inc=1, device_id=dev, device_id_type=MESH)
    pl.semaphore_wait(barrier, len(peers))

    def w_copy(way, s, sub):
        owner = (me + n_z - s + 1) % n_z if way == 0 else (me + s - 1) % n_z
        return send(
            w_buf.at[owner, sub],
            w_buf.at[owner, sub],
            w_send.at[way, s - 1, sub],
            w_recv.at[way, s - 1, sub],
            z_dev[way],
        )

    def f_copy(way, s, sub):
        owner = (me + n_z - s + 1) % n_z if way == 0 else (me + s - 1) % n_z
        return send(
            f_buf.at[owner, sub],
            f_buf.at[owner, sub],
            f_send.at[way, s - 1, sub],
            f_recv.at[way, s - 1, sub],
            z_dev[way],
        )

    for i in range(2):
        for sub in range(W_SUB):
            pltpu.make_async_copy(
                wq_ref.at[pl.ds(sub * sub_rows, sub_rows), :],
                w_buf.at[me, sub, :, pl.ds(i * heads * DK, heads * DK)],
                wload_sem.at[i, sub],
            ).wait()
    for sub in range(W_SUB):
        for way in range(2):
            w_copy(way, 1, sub).start()
    cand_load.wait()

    def a_block(part, owner):
        lanes = pl.ds(pl.multiple_of((owner * 2 + core) * mine, mine), mine)
        return a_buf.at[pl.ds(part * rows, rows), lanes]

    def a_x(part, d):
        if d == 2:
            if part == 0:
                src, dev = a_block(0, (x + n_x - 1) % n_x), x_dev[1]
            else:
                src, dev = a_block(1, (x + 1) % n_x), x_dev[n_x - 1]
        else:
            src, dev = a_block(part, x), x_dev[d]
        return send(src, src, ax_send.at[part, d], ax_recv.at[part, d], dev)

    def a_sib(part, d):
        src = a_block(part, (x + n_x - d) % n_x)
        return send(src, src, as_send.at[part, d], as_recv.at[part, d], sib_dev)

    y_copy = send(a_block(0, x), a_block(1, x), y_send, y_recv, y_dev)
    y_copy.start()
    a_x(0, 1).start()
    a_x(0, 3).start()
    a_sib(0, 0).start()

    def w_step(s):
        for sub in range(W_SUB):
            for way in range(2):
                w_copy(way, s, sub).wait_recv()
                if s < half - 1 or sub == way:
                    w_copy(way, s + 1, sub).start()

    def dot_block(owner):
        lanes = pl.ds(pl.multiple_of(owner * depth, depth), depth)
        left = n_buf[:, lanes]
        for sub in range(W_SUB):
            part = left[:, sub * sub_rows : (sub + 1) * sub_rows]
            acc[...] += jnp.dot(part, w_buf[owner, sub], preferred_element_type=F32)

    def dot_steps(lo, hi):
        @pl.loop(lo, hi)
        def _(s):
            dot_block((me + n_z - s) % n_z)
            dot_block((me + s) % n_z)

    w_step(1)
    a_x(0, 1).wait_recv()
    a_x(0, 2).start()
    a_sib(0, 1).start()
    a_x(0, 3).wait_recv()
    a_sib(0, 3).start()
    y_copy.wait_recv()
    a_x(1, 1).start()
    a_x(1, 3).start()
    a_sib(1, 0).start()
    w_step(2)
    a_x(0, 2).wait_recv()
    a_sib(0, 2).start()
    a_x(1, 3).wait_recv()
    a_x(1, 2).start()
    a_sib(1, 3).start()
    a_x(1, 1).wait_recv()
    a_sib(1, 1).start()
    w_step(3)
    a_x(1, 2).wait_recv()
    a_sib(1, 2).start()
    w_step(4)
    for part in range(2):
        for d in range(n_x):
            a_sib(part, d).wait_recv()

    strip = 64

    @pl.loop(0, 2 * rows // strip)
    def _(i):
        at = pl.ds(pl.multiple_of(i * strip, strip), strip)
        whole = a_buf[at, :].astype(F32)
        scale = lax.rsqrt(jnp.mean(whole * whole, axis=1, keepdims=True) + epsilon)
        n_buf[at, :] = (whole * scale * gain_ref[...]).astype(BF)

    w_step(5)
    side_in = mm_t(n_buf[pl.ds(0, rows), :], fb_ref[...])
    column = lax.broadcasted_iota(jnp.int32, side_in.shape, 1)
    all_heads = fb_ref.shape[0] // 2
    for h in range(heads):
        at = tp * heads + h
        decay_in = jnp.sum(jnp.where(column == at, side_in, 0.0), axis=1, keepdims=True)
        beta_in = jnp.sum(jnp.where(column == all_heads + at, side_in, 0.0), axis=1, keepdims=True)
        raised = decay_in + offset_ref[:, h : h + 1]
        soft = jnp.maximum(raised, 0.0) + jnp.log1p(jnp.exp(-jnp.abs(raised)))
        log_decay = -jnp.exp(rates_ref[:, h : h + 1]) * soft + extra_ref[:, h : h + 1]
        scal_buf[h] = jnp.broadcast_to(log_decay, (rows, DK))
        scal_buf[heads + h] = jnp.broadcast_to(jax.nn.sigmoid(beta_in), (rows, DK))
    acc[...] = jnp.zeros_like(acc)
    dot_block(me)
    dot_steps(1, 4)
    w_step(6)
    dot_steps(4, 6)
    w_step(7)
    for c in f_loads:
        c.wait()
    for sub in range(F_SUB):
        for way in range(2):
            f_copy(way, 1, sub).start()
    dot_steps(6, 8)
    for way in range(2):
        w_copy(way, half, way).wait_recv()
    dot_block((me + half) % n_z)

    for m in range(2):
        cols = slice(m * heads * DK, (m + 1) * heads * DK)
        c_send[m] = acc[pl.ds(rows, rows), cols].astype(BF)
    c_copies = [
        send(c_send.at[m], c_buf.at[side, m], c_ssem.at[m], c_rsem.at[m], y_dev) for m in range(2)
    ]
    for c in c_copies:
        c.start()
    for m in range(2):
        cols = slice(m * heads * DK, (m + 1) * heads * DK)
        c_buf[side, m] = acc[pl.ds(0, rows), cols].astype(BF)

    def f_step(s, last):
        for sub in range(F_SUB):
            for way in range(2):
                f_copy(way, s, sub).wait_recv()
                if not last or (sub * 2) // F_SUB == way:
                    f_copy(way, s + 1, sub).start()

    f_step(1, False)
    taken_load.wait()
    for m in range(2):
        send(
            c_send.at[m], c_buf.at[1 - side, m], c_ssem.at[m], c_rsem.at[m], y_dev
        ).wait_recv()
    f_step(2, False)

    for h in range(heads):
        cols = slice(h * DK, (h + 1) * DK)
        qn_buf[h] = unit_norm(c_buf[0, 0, :, cols].astype(F32)) * DK ** (-0.5)
        kn_buf[h] = unit_norm(c_buf[0, 1, :, cols].astype(F32))

    blk = 16
    per = blk // P_SIZE
    group = (lax.broadcasted_iota(jnp.int32, (2 * blk, DK), 0) % blk) // P_SIZE

    def recall(lo, hi):
        @pl.loop(lo, hi)
        def _(i):
            at = pl.ds(pl.multiple_of(i * blk, blk), blk)
            for h in range(heads):
                both = jnp.concatenate([kn_buf[h, at, :], qn_buf[h, at, :]], axis=0).astype(BF)
                picked = jnp.zeros((2 * blk, DK), F32)
                for s in range(per):
                    got = mm(both, t_buf[i * per + s, h])
                    picked = jnp.where(group == s, got, picked)
                kt_buf[h, at, :] = picked[:blk]
                qt_buf[h, at, :] = picked[blk:]

    blocks = rows // blk
    recall(0, blocks // 2)
    f_step(3, False)
    recall(blocks // 2, blocks)
    f_step(4, False)

    masks = group_masks(rows)

    def attend(h):
        cols = slice(h * DK, (h + 1) * DK)
        log_decay = scal_buf[h][:, :1]
        beta = scal_buf[heads + h][:, :1]
        summed, _, between = decay_terms(log_decay, masks)
        keys = kn_buf[h]
        fade = jnp.exp(summed)
        wanted = beta * (c_buf[1, 0, :, cols].astype(F32) - fade * kt_buf[h])
        fixes = corrections(keys, wanted, beta, between, masks)
        pairs = between * mm_t(qn_buf[h], keys)
        seen = fade * qt_buf[h] + mm(pairs, fixes)
        gate = c_buf[1, 1, :, cols].astype(F32)
        level = lax.rsqrt(jnp.mean(seen * seen, axis=1, keepdims=True) + epsilon)
        flat[:, cols] = (
            seen * level * out_gain_ref[...] * (gate * jax.nn.sigmoid(gate))
        ).astype(BF)

    for h in range(heads):
        attend(h)
    f_step(5, False)

    def slot_of(owner):
        return (owner // 4) * 2 + owner % 2

    def rs_copy(slot):
        return send(s_buf.at[slot], r_buf.at[slot], rs_send.at[slot], rs_recv.at[slot], sib_dev)

    def rx_copy(slot, dest):
        d = (dest + n_x - x) % n_x
        i = slot % 2
        return send(
            x_send.at[slot],
            x_buf.at[d - 1, i],
            rx_send.at[slot],
            rx_recv.at[d - 1, i],
            {"tp": dest * 2 + core},
        )

    def product(owner):
        slot = slot_of(owner)
        block = f_buf[owner].reshape(heads * DK, depth)
        terms = jnp.dot(flat[...], block, preferred_element_type=F32)
        kept = (owner // 2) % 2 == core

        @pl.when(kept)
        def _():
            p_buf[slot] = terms

        @pl.when(jnp.logical_not(kept))
        def _():
            s_buf[slot] = terms.astype(BF)
            rs_copy(slot).start()

    def passed_on(owner):
        slot = slot_of(owner)
        dest = owner // 4
        kept = (owner // 2) % 2 == core

        @pl.when(kept)
        def _():
            rs_copy(slot).wait_recv()

            @pl.when(dest == x)
            def _():
                own[slot % 2] = p_buf[slot] + r_buf[slot].astype(F32)

            @pl.when(dest != x)
            def _():
                x_send[slot] = (p_buf[slot] + r_buf[slot].astype(F32)).astype(BF)
                rx_copy(slot, dest).start()

    product(me)

    @pl.loop(1, 5)
    def _(s):
        product((me + n_z - s) % n_z)
        product((me + s) % n_z)
        passed_on((me + n_z - s + 1) % n_z)

        @pl.when(s > 1)
        def _():
            passed_on((me + s - 1) % n_z)

    for s in range(5, half):
        if s > 5:
            f_step(s, s == half - 1)
        product((me + n_z - s) % n_z)
        product((me + s) % n_z)
        passed_on((me + n_z - s + 1) % n_z)
        passed_on((me + s - 1) % n_z)
    for sub in range(F_SUB):
        f_copy((sub * 2) // F_SUB, half, sub).wait_recv()
    product((me + half) % n_z)
    passed_on((me + half + 1) % n_z)
    passed_on((me + half - 1) % n_z)
    passed_on((me + half) % n_z)

    for d in range(1, n_x):
        for i in range(2):
            send(
                x_send.at[i], x_buf.at[d - 1, i], rx_send.at[i], rx_recv.at[d - 1, i], x_dev[d]
            ).wait_recv()
    for i in range(2):
        total = own[i]
        for d in range(1, n_x):
            total = total + x_buf[d - 1, i].astype(F32)
        out_ref[:, i * depth : (i + 1) * depth] = total.astype(BF)

    y_copy.wait_send()
    for part in range(2):
        for d in range(1, n_x):
            a_x(part, d).wait_send()
        for d in range(n_x):
            a_sib(part, d).wait_send()
    for s in range(1, half + 1):
        for way in range(2):
            for sub in range(W_SUB):
                if s < half or sub == way:
                    w_copy(way, s, sub).wait_send()
            for sub in range(F_SUB):
                if s < half or (sub * 2) // F_SUB == way:
                    f_copy(way, s, sub).wait_send()
    for c in c_copies:
        c.wait_send()
    for slot in range(2 * n_x):
        rs_copy(slot).wait_send()

        @pl.when(slot // 2 != x)
        def _():
            rx_copy(slot, slot // 2).wait_send()


def mixed_of(mesh_sizes, operands):
    n_z, n_tp = mesh_sizes
    n_x = n_tp // 2
    (cand, gain, wq, wk, wv, wg, fb, rates, offset, extra, out_gain, proj, taken) = operands
    rows, mine = cand.shape
    width, depth = proj.shape
    heads = width // DK
    features = gain.shape[1]
    half = n_z // 2
    anywhere = pl.BlockSpec(memory_space=pl.ANY)
    held = pl.BlockSpec(memory_space=pltpu.VMEM)
    dma = pltpu.SemaphoreType.DMA
    return pl.pallas_call(
        functools.partial(mix_kernel, n_z, n_x),
        out_shape=jax.ShapeDtypeStruct((rows, mine), BF),
        in_specs=[
            anywhere,
            held,
            anywhere,
            anywhere,
            anywhere,
            anywhere,
            held,
            held,
            held,
            held,
            held,
            anywhere,
            anywhere,
        ],
        out_specs=held,
        scratch_shapes=[
            pltpu.VMEM((2 * rows, features), BF),
            pltpu.VMEM((2 * rows, features), BF),
            pltpu.VMEM((n_z, W_SUB, depth // W_SUB, 2 * width), BF),
            pltpu.VMEM((n_z, F_SUB, width // F_SUB, depth), BF),
            pltpu.VMEM(taken.shape, F32),
            pltpu.VMEM((2 * rows, 2 * width), F32),
            pltpu.VMEM((2, rows, width), BF),
            pltpu.VMEM((2, 2, rows, width), BF),
            pltpu.VMEM((heads, rows, DK), F32),
            pltpu.VMEM((heads, rows, DK), F32),
            pltpu.VMEM((heads, rows, DK), F32),
            pltpu.VMEM((heads, rows, DK), F32),
            pltpu.VMEM((2 * heads, rows, DK), F32),
            pltpu.VMEM((rows, width), BF),
            pltpu.VMEM((2 * n_x, rows, depth), F32),
            pltpu.VMEM((2 * n_x, rows, depth), BF),
            pltpu.VMEM((2 * n_x, rows, depth), BF),
            pltpu.VMEM((2 * n_x, rows, depth), BF),
            pltpu.VMEM((n_x - 1, 2, rows, depth), BF),
            pltpu.VMEM((2, rows, depth), F32),
            dma((2 + F_SUB,)),
            dma((2, W_SUB)),
            dma,
            dma,
            dma((2, n_x)),
            dma((2, n_x)),
            dma((2, n_x)),
            dma((2, n_x)),
            dma((2, half, W_SUB)),
            dma((2, half, W_SUB)),
            dma((2, half, F_SUB)),
            dma((2, half, F_SUB)),
            dma((2,)),
            dma((2,)),
            dma((2 * n_x,)),
            dma((2 * n_x,)),
            dma((2 * n_x,)),
            dma((n_x - 1, 2)),
        ],
        compiler_params=pltpu.CompilerParams(collective_id=0, has_side_effects=True),
        cost_estimate=pl.CostEstimate(
            flops=4 * rows * features * 2 * width, bytes_accessed=1 << 24, transcendentals=0
        ),
    )(cand, gain, wq, wk, wv, wg, fb, rates, offset, extra, out_gain, proj, taken)


def on_device(
    mesh_sizes,
    candidate_embeddings,
    incoming_rms_scaling,
    probe_projector,
    address_projector,
    content_projector,
    sigmoid_mask_matrix,
    forgetting_projector,
    strength_projector_matrix,
    channel_forgetting_rates,
    forgetting_offset,
    extra_forgetting,
    outgoing_rms_scaling,
    final_projector,
    memory_matrix,
    earlier_addresses,
    earlier_contents,
    earlier_strengths,
    earlier_forgetting,
    admitted_counts,
):
    rows = candidate_embeddings.shape[0]
    heads = memory_matrix.shape[1]
    live = (admitted_counts[:, None] > jnp.arange(P_SIZE)[None, :])[..., None]
    scalars = jnp.concatenate(
        [jnp.where(live, earlier_strengths, 0.0), jnp.where(live, earlier_forgetting, 0.0)], axis=-1
    ).reshape(rows, 2 * heads)
    taken = taken_state_of(
        earlier_addresses.reshape(rows, heads * DK),
        earlier_contents.reshape(rows, heads * DK),
        scalars,
        memory_matrix,
    )
    side_weights = jnp.concatenate([forgetting_projector, strength_projector_matrix], axis=1).T
    mixed = mixed_of(
        mesh_sizes,
        (
            candidate_embeddings,
            incoming_rms_scaling[None, :],
            probe_projector,
            address_projector,
            content_projector,
            sigmoid_mask_matrix,
            side_weights,
            channel_forgetting_rates[None, :],
            forgetting_offset[None, :],
            extra_forgetting.reshape(rows, heads),
            outgoing_rms_scaling[None, :],
            final_projector,
            taken,
        ),
    )
    return (mixed, taken)


def solution(mesh):
    in_specs = (
        P(("grp", "kv"), "tp"),
        P(),
        P("kv", "tp"),
        P("kv", "tp"),
        P("kv", "tp"),
        P("kv", "tp"),
        P(),
        P(),
        P("tp"),
        P("tp"),
        P(("grp", "kv"), None, "tp"),
        P(),
        P("tp", "kv"),
        P(("grp", "kv"), "tp", None, None),
        P(("grp", "kv"), None, "tp", None),
        P(("grp", "kv"), None, "tp", None),
        P(("grp", "kv"), None, "tp"),
        P(("grp", "kv"), None, "tp"),
        P(("grp", "kv")),
    )
    out_specs = (P(("grp", "kv"), "tp"), P(("grp", "kv"), "tp", None, None))
    sizes = (mesh.shape["kv"], mesh.shape["tp"])
    return jax.shard_map(
        functools.partial(on_device, sizes),
        mesh=mesh,
        in_specs=in_specs,
        out_specs=out_specs,
        check_vma=False,
    )
```

time: 242 us -> 132 us (0.55); the launches traced: 238 us -> 131 us
  Pallas kernels: 0 us -> 124 us
  matrix products: 88.2 us -> 0 us
  waiting for transfers between devices: 54.5 us -> 0 us
  blocking collectives: 23.3 us -> 0 us
  starting transfers between devices: 22.8 us -> 0 us
  other arithmetic: 21.7 us -> 2.09 us
  between operations: 14.6 us -> 0.65 us
  local copies, waits for them, and re-layouts: 13.3 us -> 4.77 us
    pallas_call x0 -> x2, Pallas kernels: none -> 124 us  [the longest x1 112 us: mixed_of(): pl.pallas_call(functools.partial(mix_kernel, n_z, n_x), out_shape=jax.Sha...]
    dot_general x19 -> x0, matrix products: 88.2 us -> none  [the longest x8 44.3 us: update(): recalled = jnp.einsum('shde,shd->she', decayed, key_vec)]
    all_gather x2 -> x0, waiting for transfers between devices: 53.7 us -> none  [the longest x1 41.4 us: side_by_side(): lax.all_gather(both, axis, axis=dim, tiled=True)]
    all_to_all x1 -> x0, blocking collectives: 23.3 us -> none  [summed_on_arrival(): blocks = lax.all_to_all(split_up(shard, dim, count), axis, 0, 0, tiled=True)]
    all_to_all x1 -> x0, starting transfers between devices: 22.8 us -> none  [sent_to_all(): lax.all_to_all(jnp.broadcast_to(shard[None], (count, *shard.shape)), axis...]
    select_n x1, other arithmetic: 11.2 us -> 0.71 us  [on_device(): jnp.where(live, earlier_strengths, 0.0)]
    convert_element_type x3 -> x0, local copies, waits for them, and re-layouts: 8.02 us -> none  [on_device(): whole = gathered_copies(candidate_embeddings, 'tp', 1).astype(jnp.float32)]
    convert_element_type x3 -> x0, other arithmetic: 3.66 us -> none  [the longest x1 2.22 us: on_device(): whole = gathered_copies(candidate_embeddings, 'tp', 1).astype(jnp.float32)]
  transfers between devices with their start and end apart: 3 -> 0, of which waited for: 2 -> 0; matrix products, arithmetic and copies ran while one was open for 49% -> 0% of each run, Pallas kernels for 0% -> 0%
where the time goes in v1:
time: 132 us; the launch traced here: 131 us
  Pallas kernels  124 us (94%)
  local copies, waits for them, and re-layouts  4.77 us (4%)
  other arithmetic  2.09 us (2%)
    pallas_call x1, Pallas kernels, mixed_of(): pl.pallas_call(functools.partial(mix_kernel, n_z, n_x), out_shape=jax.Sha...  112 us
    pallas_call x1, Pallas kernels, taken_state_of(): pl.pallas_call(taken_kernel, grid=(seqs // block,), in_specs=[pl.BlockSpe...  11.7 us

profile of v1, /device:TPU:36, one launch (start us, length us, event | category | flops | bytes accessed | tf_op | source)
XLA Modules:
  0.0 131.4 jit_solution(6636678908001684361)
XLA Ops:
  0.6 0.7 iota_compare_fusion
  1.3 0.7 broadcast_select_fusion.1
  2.0 0.8 copy.22
  2.8 1.6 %copy_bitcast_fusion = (bf16[192,256]{1,0:T(8,128)(2,1)}, bf16[192,256]{1,0:T(8,128)(2,1)}) fusion(bf16[24,8,2,128]{3,2,1,0:T(2,128)(2,1)} %bitcast.18, bf16[24,8,2,128]{3,2,1,0:T(2,128)(2,1)} %bitcast.19), kind=kLoop, calls=%fused_computation.1 | loop fusion | bytes 393216 | tf_op jit(solution)/shard_map/reshape | solution.py:672
  4.4 0.0 copy-start
  4.4 0.0 copy-start.1
  4.4 0.0 copy-start.2
  4.4 11.7 %shard_map.194.taken_ref = f32[48,2,128,128]{3,2,1,0:T(8,128)} custom-call(bf16[192,256]{1,0:T(8,128)(2,1)} %get-tuple-element.5.keys_ref, bf16[192,256]{1,0:T(8,128)(2,1)} %get-tuple-element.4.values_ref, f32[192,4]{1,0:T(8,128)} %bitcast.17, f32[48,2,128,128]{3,2,1,0:T(8,128)} %state_ref.1), custom_call_target="tpu_custom_call" | custom-call | flops 50331648 | bytes 12582912 | tf_op jit(solution)/shard_map/pallas_call | solution.py:90
  16.1 0.0 copy-done
  16.1 0.0 copy-done.1
  16.1 0.7 maximum_bitcast_fusion.fb_ref
  16.8 0.0 copy-done.2
  16.8 0.8 copy.21
  17.6 112.2 %shard_map.195 = bf16[192,512]{1,0:T(8,128)(2,1)} custom-call(bf16[192,512]{1,0:T(8,128)(2,1)} %cand_ref.1, f32[1,4096]{1,0:T(1,128)} %bitcast.20, bf16[256,256]{1,0:T(8,128)(2,1)} %wq_ref.1, bf16[256,256]{1,0:T(8,128)(2,1)} %wk_ref.1, bf16[256,256]{1,0:T(8,128)(2,1)} %wv_ref.1, bf16[256,256]{1,0:T(8,128)(2,1)} %wg_ref.1, ...), custom_call_target="tpu_custom_call" | custom-call | flops 1610612736 | bytes 16777216 | tf_op jit(solution)/shard_map/pallas_call | solution.py:576
  129.8 1.6 %copy.28 = bf16[192,512]{1,0:T(8,128)(2,1)} copy(bf16[192,512]{1,0:T(8,128)(2,1)} %shard_map.195) | data formatting | bytes 393216
  (1 shorter events, 0.0 us)
Async XLA Ops:
  4.4 11.7 %copy-start = (bf16[4096,16]{0,1:T(8,128)(2,1)S(1)}, bf16[4096,16]{0,1:T(8,128)(2,1)}, u32[]{:S(2)}) copy-start(bf16[4096,16]{0,1:T(8,128)(2,1)} %param.26) | copy-start | bytes 393220
  4.4 11.7 %copy-start.1 = (bf16[4096,16]{0,1:T(8,128)(2,1)S(1)}, bf16[4096,16]{0,1:T(8,128)(2,1)}, u32[]{:S(2)}) copy-start(bf16[4096,16]{0,1:T(8,128)(2,1)} %param.25) | copy-start | bytes 393220
  4.4 12.4 %copy-start.2 = (f32[48,4,2]{0,2,1:T(2,128)S(1)}, f32[48,4,2]{0,2,1:T(2,128)}, u32[]{:S(2)}) copy-start(f32[48,4,2]{0,2,1:T(2,128)} %param.29) | copy-start | bytes 4612

commit v2 on v1

v2 whole, which is shorter than its diff:
```python
import functools

import jax
import jax.numpy as jnp
from jax import lax
from jax.experimental import pallas as pl
from jax.experimental.pallas import tpu as pltpu
from jax.sharding import PartitionSpec as P

DK = 128
P_SIZE = 4
W_SUB = 4
F_SUB = 4
VMEM_BYTES = 67043328

epsilon = 1e-06
MESH = pl.DeviceIdType.MESH
BF = jnp.bfloat16
F32 = jnp.float32


def unit_norm(vector):
    return vector * lax.rsqrt(jnp.sum(vector * vector, axis=-1, keepdims=True) + epsilon)


def mm(a, b):
    return jnp.dot(a.astype(BF), b.astype(BF), preferred_element_type=F32)


def mm_t(a, b):
    return lax.dot_general(
        a.astype(BF), b.astype(BF), (((1,), (1,)), ((), ())), preferred_element_type=F32
    )


def group_masks(count, heads):
    row = lax.broadcasted_iota(jnp.int32, (count, count), 0)
    col = lax.broadcasted_iota(jnp.int32, (count, count), 1)
    span = P_SIZE * heads
    same = (row // span == col // span) & (row % heads == col % heads)
    return row == col, same, same & (col <= row), same & (col < row)


def decay_terms(log_decay, masks):
    eye, same, upto, _ = masks
    along = jnp.sum(jnp.where(eye, log_decay, 0.0), axis=0, keepdims=True)
    summed = jnp.sum(jnp.where(upto, along, 0.0), axis=1, keepdims=True)
    total = jnp.sum(jnp.where(same, along, 0.0), axis=1, keepdims=True)
    summed_along = jnp.sum(jnp.where(eye, summed, 0.0), axis=0, keepdims=True)
    between = jnp.exp(jnp.where(upto, summed - summed_along, -1e30))
    return summed, total, between


def corrections(keys, wanted, beta, between, masks):
    lower = jnp.where(masks[3], beta * between * mm_t(keys, keys), 0.0)
    both = wanted + mm(lower, mm(lower, wanted))
    return both - mm(lower, both)


def columns(lines, count):
    period = len(lines)
    shape = (count, lines[0].shape[1])
    row = lax.broadcasted_iota(jnp.int32, shape, 0)
    col = lax.broadcasted_iota(jnp.int32, shape, 1)
    spread = jnp.zeros(shape, F32)
    for a, line in enumerate(lines):
        spread = jnp.where(row % period == a, line, spread)
    return jnp.sum(jnp.where(col == row // period, spread, 0.0), axis=1, keepdims=True)


def mix_kernel(
    n_z,
    n_x,
    cand_ref,
    gain_far,
    wq_ref,
    wk_ref,
    wv_ref,
    wg_ref,
    decay_w_far,
    beta_w_far,
    rates_far,
    offset_far,
    extra_far,
    out_gain_far,
    proj_ref,
    state_ref,
    old_keys_far,
    old_values_far,
    old_beta_far,
    old_decay_far,
    counts_far,
    out_ref,
    t_buf,
    gain_ref,
    decay_w_ref,
    beta_w_ref,
    rates_ref,
    offset_ref,
    extra_ref,
    out_gain_ref,
    old_keys_ref,
    old_values_ref,
    old_beta_ref,
    old_decay_ref,
    counts_ref,
    a_buf,
    n_buf,
    w_buf,
    f_buf,
    acc,
    c_send,
    c_buf,
    kn_buf,
    qn_buf,
    kt_buf,
    qt_buf,
    scal_buf,
    old_scal,
    old_unit,
    old_seen,
    old_fix,
    flat,
    p_buf,
    s_buf,
    r_buf,
    x_send,
    x_buf,
    own,
    local_sem,
    small_sem,
    wload_sem,
    y_send,
    y_recv,
    ax_send,
    ax_recv,
    as_send,
    as_recv,
    w_send,
    w_recv,
    f_send,
    f_recv,
    c_ssem,
    c_rsem,
    rs_send,
    rs_recv,
    rx_send,
    rx_recv,
):
    rows, mine = cand_ref.shape
    width, depth = proj_ref.shape
    heads = width // DK
    half = n_z // 2
    tp = lax.axis_index("tp")
    me = lax.axis_index("kv")
    grp = lax.axis_index("grp")
    x = tp // 2
    core = tp % 2
    side = grp % 2
    z_dev = ({"kv": (me + 1) % n_z}, {"kv": (me + n_z - 1) % n_z})
    y_dev = {"grp": grp + 1 - 2 * side}
    x_dev = [{"tp": ((x + d) % n_x) * 2 + core} for d in range(n_x)]
    sib_dev = {"tp": x * 2 + 1 - core}

    def send(src, dst, s_sem, r_sem, dev):
        return pltpu.make_async_remote_copy(
            src_ref=src,
            dst_ref=dst,
            send_sem=s_sem,
            recv_sem=r_sem,
            device_id=dev,
            device_id_type=MESH,
        )

    def w_load(ref, i):
        return pltpu.make_async_copy(
            ref, w_buf.at[me, :, pl.ds(i * width, width)], wload_sem.at[i]
        )

    @pl.when(side == 0)
    def _():
        w_load(wq_ref, 0).start()
        w_load(wk_ref, 1).start()

    @pl.when(side == 1)
    def _():
        w_load(wv_ref, 0).start()
        w_load(wg_ref, 1).start()

    cand_load = pltpu.make_async_copy(
        cand_ref, a_buf.at[pl.ds(0, rows), pl.ds(pl.multiple_of(tp * mine, mine), mine)], local_sem.at[0]
    )
    cand_load.start()
    f_load = pltpu.make_async_copy(proj_ref, f_buf.at[me], local_sem.at[1])
    f_load.start()
    state_load = pltpu.make_async_copy(state_ref, t_buf, local_sem.at[2])
    state_load.start()
    small = (
        (gain_far, gain_ref),
        (decay_w_far, decay_w_ref),
        (beta_w_far, beta_w_ref),
        (rates_far, rates_ref),
        (offset_far, offset_ref),
        (extra_far, extra_ref),
        (out_gain_far, out_gain_ref),
        (old_keys_far, old_keys_ref),
        (old_values_far, old_values_ref),
        (old_beta_far, old_beta_ref),
        (old_decay_far, old_decay_ref),
        (counts_far, counts_ref),
    )
    small_loads = [
        pltpu.make_async_copy(src, dst, small_sem.at[i])
        for i, (src, dst) in enumerate(small)
    ]
    for c in small_loads:
        c.start()

    barrier = pltpu.get_barrier_semaphore()
    peers = (z_dev[0], z_dev[1], y_dev, sib_dev, *x_dev[1:])
    for dev in peers:
        pl.semaphore_signal(barrier, inc=1, device_id=dev, device_id_type=MESH)
    pl.semaphore_wait(barrier, len(peers))

    def ring_copy(buf, subs, s_sems, r_sems, way, s, sub):
        owner = (me + n_z - s + 1) % n_z if way == 0 else (me + s - 1) % n_z
        size = buf.shape[1] // subs
        part = buf.at[owner, pl.ds(sub * size, size), :]
        return send(
            part, part, s_sems.at[way, s - 1, sub], r_sems.at[way, s - 1, sub], z_dev[way]
        )

    def w_copy(way, s, sub):
        return ring_copy(w_buf, W_SUB, w_send, w_recv, way, s, sub)

    def f_copy(way, s, sub):
        return ring_copy(f_buf, F_SUB, f_send, f_recv, way, s, sub)

    def goes(subs, way, s, sub):
        return s < half or (sub * 2) // subs == way

    w_load(wq_ref, 0).wait()
    w_load(wk_ref, 1).wait()
    for sub in range(W_SUB):
        for way in range(2):
            w_copy(way, 1, sub).start()
    cand_load.wait()

    def a_block(part, owner):
        lanes = pl.ds(pl.multiple_of((owner * 2 + core) * mine, mine), mine)
        return a_buf.at[pl.ds(part * rows, rows), lanes]

    def a_x(part, d):
        if d == 2:
            if part == 0:
                src, dev = a_block(0, (x + n_x - 1) % n_x), x_dev[1]
            else:
                src, dev = a_block(1, (x + 1) % n_x), x_dev[n_x - 1]
        else:
            src, dev = a_block(part, x), x_dev[d]
        return send(src, src, ax_send.at[part, d], ax_recv.at[part, d], dev)

    def a_sib(part, d):
        src = a_block(part, (x + n_x - d) % n_x)
        return send(src, src, as_send.at[part, d], as_recv.at[part, d], sib_dev)

    y_copy = send(a_block(0, x), a_block(1, x), y_send, y_recv, y_dev)
    y_copy.start()
    a_x(0, 1).start()
    a_x(0, 3).start()
    a_sib(0, 0).start()

    def w_event(s, sub):
        for way in range(2):
            if goes(W_SUB, way, s, sub):
                w_copy(way, s, sub).wait_recv()
                if s < half and goes(W_SUB, way, s + 1, sub):
                    w_copy(way, s + 1, sub).start()

    def f_step(s):
        for sub in range(F_SUB):
            for way in range(2):
                if goes(F_SUB, way, s, sub):
                    f_copy(way, s, sub).wait_recv()
                    if s < half and goes(F_SUB, way, s + 1, sub):
                        f_copy(way, s + 1, sub).start()

    span = P_SIZE * heads
    old_rows = old_keys_ref.shape[0]
    oblk = 32
    oper = oblk // span
    oblocks = old_rows // oblk
    orow = lax.broadcasted_iota(jnp.int32, (oblk, DK), 0)

    def old_scalars():
        counts = counts_ref[...]
        betas, decays = [], []
        for j in range(P_SIZE):
            for h in range(heads):
                live = counts > j
                betas.append(jnp.where(live, old_beta_ref[j, h : h + 1, :], 0.0))
                decays.append(jnp.where(live, old_decay_ref[j, h : h + 1, :], 0.0))
        old_scal[0] = columns(betas, old_rows)
        old_scal[1] = columns(decays, old_rows)

    def old_recall(lo, hi):
        @pl.loop(lo, hi)
        def _(i):
            at = pl.ds(pl.multiple_of(i * oblk, oblk), oblk)
            keys = unit_norm(old_keys_ref[at, :].astype(F32))
            old_unit[at, :] = keys
            picked = jnp.zeros((oblk, DK), F32)
            for s in range(oper):
                for h in range(heads):
                    hit = (orow // span == s) & (orow % heads == h)
                    picked = jnp.where(hit, mm(keys, t_buf[i * oper + s, h]), picked)
            old_seen[at, :] = picked

    ochunk = 128

    def old_solve(c):
        at = pl.ds(c * ochunk, ochunk)
        masks = group_masks(ochunk, heads)
        beta, log_decay = old_scal[0, at, :], old_scal[1, at, :]
        summed, total, between = decay_terms(log_decay, masks)
        keys = old_unit[at, :]
        values = old_values_ref[at, :].astype(F32)
        wanted = beta * (values - jnp.exp(summed) * old_seen[at, :])
        fixes = corrections(keys, wanted, beta, between, masks)
        old_fix[at, :] = jnp.exp(total - summed) * fixes
        old_scal[2, at, :] = jnp.exp(total)

    def old_apply(lo, hi):
        @pl.loop(lo, hi)
        def _(i):
            at = pl.ds(pl.multiple_of(i * oblk, oblk), oblk)
            fixes = old_fix[at, :]
            kept = old_scal[2, at, :]
            spread = [
                jnp.where((orow // span == s) & (orow % heads == h), fixes, 0.0)
                for s in range(oper)
                for h in range(heads)
            ]
            added = lax.dot_general(
                old_unit[at, :].astype(BF),
                jnp.concatenate(spread, axis=1).astype(BF),
                (((0,), (0,)), ((), ())),
                preferred_element_type=F32,
            )
            for s in range(oper):
                for h in range(heads):
                    scale = kept[s * span + h : s * span + h + 1, :]
                    lanes = slice((s * heads + h) * DK, (s * heads + h + 1) * DK)
                    t_buf[i * oper + s, h] = scale * t_buf[i * oper + s, h] + added[:, lanes]

    strip = 16
    strips = 2 * rows // strip

    def norm(lo, hi):
        @pl.loop(lo, hi)
        def _(i):
            at = pl.ds(pl.multiple_of(i * strip, strip), strip)
            whole = a_buf[at, :].astype(F32)
            scale = lax.rsqrt(jnp.mean(whole * whole, axis=1, keepdims=True) + epsilon)
            n_buf[at, :] = (whole * scale * gain_ref[...]).astype(BF)

    def side_inputs():
        left = n_buf[pl.ds(0, rows), :]
        decay_ins = mm_t(left, decay_w_ref[...])
        beta_ins = mm_t(left, beta_w_ref[...])
        column = lax.broadcasted_iota(jnp.int32, decay_ins.shape, 1)
        for h in range(heads):
            here = column == tp * heads + h
            decay_in = jnp.sum(jnp.where(here, decay_ins, 0.0), axis=1, keepdims=True)
            beta_in = jnp.sum(jnp.where(here, beta_ins, 0.0), axis=1, keepdims=True)
            raised = decay_in + offset_ref[:, h : h + 1]
            soft = jnp.maximum(raised, 0.0) + jnp.log1p(jnp.exp(-jnp.abs(raised)))
            extra = columns([extra_ref[t, h : h + 1, :] for t in range(P_SIZE)], rows)
            scal_buf[h] = -jnp.exp(rates_ref[:, h : h + 1]) * soft + extra
            scal_buf[heads + h] = jax.nn.sigmoid(beta_in)

    def dot_block(owner):
        lanes = pl.ds(pl.multiple_of(owner * depth, depth), depth)
        acc[...] += jnp.dot(n_buf[:, lanes], w_buf[owner], preferred_element_type=F32)

    def dot_first():
        lanes = pl.ds(pl.multiple_of(me * depth, depth), depth)
        acc[...] = jnp.dot(n_buf[:, lanes], w_buf[me], preferred_element_type=F32)

    def dot_steps(lo, hi):
        @pl.loop(lo, hi)
        def _(s):
            dot_block((me + n_z - s) % n_z)
            dot_block((me + s) % n_z)

    def a_first():
        a_x(0, 1).wait_recv()
        a_x(0, 2).start()
        a_sib(0, 1).start()
        a_x(0, 3).wait_recv()
        a_sib(0, 3).start()

    def a_paired():
        y_copy.wait_recv()
        a_x(1, 1).start()
        a_x(1, 3).start()
        a_sib(1, 0).start()

    def a_second():
        a_x(0, 2).wait_recv()
        a_sib(0, 2).start()
        a_x(1, 3).wait_recv()
        a_x(1, 2).start()
        a_sib(1, 3).start()
        a_x(1, 1).wait_recv()
        a_sib(1, 1).start()

    def a_third():
        a_x(1, 2).wait_recv()
        a_sib(1, 2).start()

    def a_last():
        for part in range(2):
            for d in range(n_x):
                a_sib(part, d).wait_recv()

    def f_begin():
        f_load.wait()
        for sub in range(F_SUB):
            for way in range(2):
                f_copy(way, 1, sub).start()

    plan = {
        (1, 1): [a_first],
        (1, 2): [functools.partial(old_recall, 4, 8)],
        (1, 3): [a_paired, functools.partial(old_recall, 8, 12)],
        (2, 0): [functools.partial(old_solve, 0)],
        (2, 1): [functools.partial(old_solve, 1)],
        (2, 2): [functools.partial(old_solve, 2)],
        (2, 3): [a_second],
        (3, 0): [functools.partial(old_apply, 0, 3)],
        (3, 1): [functools.partial(old_apply, 3, 6)],
        (3, 2): [functools.partial(old_apply, 6, 9)],
        (3, 3): [a_third],
        (4, 0): [functools.partial(old_apply, 9, 12)],
        (4, 2): [a_last, functools.partial(norm, 0, 4)],
        (4, 3): [functools.partial(norm, 4, 8)],
        (5, 0): [functools.partial(norm, 8, 12)],
        (5, 1): [functools.partial(norm, 12, 16)],
        (5, 2): [functools.partial(norm, 16, 20)],
        (5, 3): [functools.partial(norm, 20, strips)],
        (6, 0): [side_inputs],
        (6, 1): [dot_first, functools.partial(dot_steps, 1, 2)],
        (6, 2): [functools.partial(dot_steps, 2, 3)],
        (6, 3): [f_begin, functools.partial(dot_steps, 3, 4)],
        (7, 0): [functools.partial(dot_steps, 4, 5)],
        (7, 1): [functools.partial(dot_steps, 5, 6)],
        (7, 2): [functools.partial(dot_steps, 6, 7)],
    }
    for c in small_loads:
        c.wait()
    old_scalars()
    state_load.wait()
    old_recall(0, 4)
    for s in range(1, half):
        for sub in range(W_SUB):
            w_event(s, sub)
            for work in plan.get((s, sub), []):
                work()
    f_step(1)
    dot_steps(half - 1, half)
    for sub in range(W_SUB):
        w_event(half, sub)
    dot_block((me + half) % n_z)

    for m in range(2):
        c_send[m] = acc[pl.ds(rows, rows), m * width : (m + 1) * width].astype(BF)
    c_copies = [
        send(c_send.at[m], c_buf.at[side, m], c_ssem.at[m], c_rsem.at[m], y_dev) for m in range(2)
    ]
    for c in c_copies:
        c.start()
    for m in range(2):
        c_buf[side, m] = acc[pl.ds(0, rows), m * width : (m + 1) * width].astype(BF)

    f_step(2)
    f_step(3)
    for c in c_copies:
        c.wait_recv()

    for h in range(heads):
        cols = slice(h * DK, (h + 1) * DK)
        qn_buf[h] = unit_norm(c_buf[0, 0, :, cols].astype(F32)) * DK ** (-0.5)
        kn_buf[h] = unit_norm(c_buf[0, 1, :, cols].astype(F32))

    blk = 16
    per = blk // P_SIZE
    group = (lax.broadcasted_iota(jnp.int32, (2 * blk, DK), 0) % blk) // P_SIZE

    def recall(lo, hi):
        @pl.loop(lo, hi)
        def _(i):
            at = pl.ds(pl.multiple_of(i * blk, blk), blk)
            for h in range(heads):
                both = jnp.concatenate([kn_buf[h, at, :], qn_buf[h, at, :]], axis=0).astype(BF)
                picked = jnp.zeros((2 * blk, DK), F32)
                for s in range(per):
                    got = mm(both, t_buf[i * per + s, h])
                    picked = jnp.where(group == s, got, picked)
                kt_buf[h, at, :] = picked[:blk]
                qt_buf[h, at, :] = picked[blk:]

    blocks = rows // blk
    recall(0, blocks // 2)
    f_step(4)
    recall(blocks // 2, blocks)

    masks = group_masks(rows, 1)

    def attend(h):
        cols = slice(h * DK, (h + 1) * DK)
        summed, _, between = decay_terms(scal_buf[h], masks)
        beta = scal_buf[heads + h]
        keys = kn_buf[h]
        fade = jnp.exp(summed)
        wanted = beta * (c_buf[1, 0, :, cols].astype(F32) - fade * kt_buf[h])
        fixes = corrections(keys, wanted, beta, between, masks)
        pairs = between * mm_t(qn_buf[h], keys)
        seen = fade * qt_buf[h] + mm(pairs, fixes)
        gate = c_buf[1, 1, :, cols].astype(F32)
        level = lax.rsqrt(jnp.mean(seen * seen, axis=1, keepdims=True) + epsilon)
        flat[:, cols] = (
            seen * level * out_gain_ref[...] * (gate * jax.nn.sigmoid(gate))
        ).astype(BF)

    for h in range(heads):
        attend(h)
    f_step(5)

    def slot_of(owner):
        return (owner // 4) * 2 + owner % 2

    def rs_copy(slot):
        return send(s_buf.at[slot], r_buf.at[slot], rs_send.at[slot], rs_recv.at[slot], sib_dev)

    def rx_copy(slot, dest):
        d = (dest + n_x - x) % n_x
        i = slot % 2
        return send(
            x_send.at[slot],
            x_buf.at[d - 1, i],
            rx_send.at[slot],
            rx_recv.at[d - 1, i],
            {"tp": dest * 2 + core},
        )

    def product(owner):
        slot = slot_of(owner)
        terms = jnp.dot(flat[...], f_buf[owner], preferred_element_type=F32)
        kept = (owner // 2) % 2 == core

        @pl.when(kept)
        def _():
            p_buf[slot] = terms

        @pl.when(jnp.logical_not(kept))
        def _():
            s_buf[slot] = terms.astype(BF)
            rs_copy(slot).start()

    def passed_on(owner):
        slot = slot_of(owner)
        dest = owner // 4
        kept = (owner // 2) % 2 == core

        @pl.when(kept)
        def _():
            rs_copy(slot).wait_recv()

            @pl.when(dest == x)
            def _():
                own[slot % 2] = p_buf[slot] + r_buf[slot].astype(F32)

            @pl.when(dest != x)
            def _():
                x_send[slot] = (p_buf[slot] + r_buf[slot].astype(F32)).astype(BF)
                rx_copy(slot, dest).start()

    product(me)

    @pl.loop(1, 5)
    def _(s):
        product((me + n_z - s) % n_z)
        product((me + s) % n_z)
        passed_on((me + n_z - s + 1) % n_z)

        @pl.when(s > 1)
        def _():
            passed_on((me + s - 1) % n_z)

    for s in range(5, half):
        if s > 5:
            f_step(s)
        product((me + n_z - s) % n_z)
        product((me + s) % n_z)
        passed_on((me + n_z - s + 1) % n_z)
        passed_on((me + s - 1) % n_z)
    f_step(half)
    product((me + half) % n_z)
    passed_on((me + half + 1) % n_z)
    passed_on((me + half - 1) % n_z)
    passed_on((me + half) % n_z)

    for d in range(1, n_x):
        for i in range(2):
            send(
                x_send.at[i], x_buf.at[d - 1, i], rx_send.at[i], rx_recv.at[d - 1, i], x_dev[d]
            ).wait_recv()
    for i in range(2):
        total = own[i]
        for d in range(1, n_x):
            total = total + x_buf[d - 1, i].astype(F32)
        out_ref[:, i * depth : (i + 1) * depth] = total.astype(BF)

    y_copy.wait_send()
    for part in range(2):
        for d in range(1, n_x):
            a_x(part, d).wait_send()
        for d in range(n_x):
            a_sib(part, d).wait_send()
    for s in range(1, half + 1):
        for way in range(2):
            for sub in range(W_SUB):
                if goes(W_SUB, way, s, sub):
                    w_copy(way, s, sub).wait_send()
            for sub in range(F_SUB):
                if goes(F_SUB, way, s, sub):
                    f_copy(way, s, sub).wait_send()
    for c in c_copies:
        c.wait_send()
    for slot in range(2 * n_x):
        rs_copy(slot).wait_send()

        @pl.when(slot // 2 != x)
        def _():
            rx_copy(slot, slot // 2).wait_send()


def layer(mesh_sizes, operands):
    n_z, n_tp = mesh_sizes
    n_x = n_tp // 2
    rows, mine = operands[0].shape
    features = operands[1].shape[1]
    width, depth = operands[12].shape
    state = operands[13]
    heads = width // DK
    half = n_z // 2
    room = VMEM_BYTES - state.size * 4 - rows * mine * 2 - (12000 << 10)
    held = pl.BlockSpec(memory_space=pltpu.VMEM)
    small = (1, 6, 7, 8, 9, 10, 11, 14, 15, 16, 17, 18)
    dma = pltpu.SemaphoreType.DMA
    return pl.pallas_call(
        functools.partial(mix_kernel, n_z, n_x),
        out_shape=(
            jax.ShapeDtypeStruct((rows, mine), BF),
            jax.ShapeDtypeStruct(state.shape, F32),
        ),
        in_specs=[pl.BlockSpec(memory_space=pltpu.HBM)] * len(operands),
        out_specs=(held, held),
        scratch_shapes=[
            *(pltpu.VMEM(operands[i].shape, operands[i].dtype) for i in small),
            pltpu.VMEM((2 * rows, features), BF),
            pltpu.VMEM((2 * rows, features), BF),
            pltpu.VMEM((n_z, depth, 2 * width), BF),
            pltpu.VMEM((n_z, width, depth), BF),
            pltpu.VMEM((2 * rows, 2 * width), F32),
            pltpu.VMEM((2, rows, width), BF),
            pltpu.VMEM((2, 2, rows, width), BF),
            pltpu.VMEM((heads, rows, DK), F32),
            pltpu.VMEM((heads, rows, DK), F32),
            pltpu.VMEM((heads, rows, DK), F32),
            pltpu.VMEM((heads, rows, DK), F32),
            pltpu.VMEM((2 * heads, rows, 1), F32),
            pltpu.VMEM((3, heads * rows, 1), F32),
            pltpu.VMEM((heads * rows, DK), F32),
            pltpu.VMEM((heads * rows, DK), F32),
            pltpu.VMEM((heads * rows, DK), F32),
            pltpu.VMEM((rows, width), BF),
            pltpu.VMEM((2 * n_x, rows, depth), F32),
            pltpu.VMEM((2 * n_x, rows, depth), BF),
            pltpu.VMEM((2 * n_x, rows, depth), BF),
            pltpu.VMEM((2 * n_x, rows, depth), BF),
            pltpu.VMEM((n_x - 1, 2, rows, depth), BF),
            pltpu.VMEM((2, rows, depth), F32),
            dma((3,)),
            dma((len(small),)),
            dma((2,)),
            dma,
            dma,
            dma((2, n_x)),
            dma((2, n_x)),
            dma((2, n_x)),
            dma((2, n_x)),
            dma((2, half, W_SUB)),
            dma((2, half, W_SUB)),
            dma((2, half, F_SUB)),
            dma((2, half, F_SUB)),
            dma((2,)),
            dma((2,)),
            dma((2 * n_x,)),
            dma((2 * n_x,)),
            dma((2 * n_x,)),
            dma((n_x - 1, 2)),
        ],
        compiler_params=pltpu.CompilerParams(
            collective_id=0, has_side_effects=True, vmem_limit_bytes=room
        ),
        cost_estimate=pl.CostEstimate(
            flops=4 * rows * features * 2 * width, bytes_accessed=1 << 24, transcendentals=0
        ),
    )(*(pltpu.with_memory_space_constraint(v, pltpu.HBM) for v in operands))


def hand_over_kernel(mixed_ref, taken_ref, mixed_out_ref, taken_out_ref, sems):
    copies = [
        pltpu.make_async_copy(taken_ref, taken_out_ref, sems.at[0]),
        pltpu.make_async_copy(mixed_ref, mixed_out_ref, sems.at[1]),
    ]
    for c in copies:
        c.start()
    for c in copies:
        c.wait()


def handed_over(mixed, taken):
    held = pl.BlockSpec(memory_space=pltpu.VMEM)
    anywhere = pl.BlockSpec(memory_space=pl.ANY)
    return pl.pallas_call(
        hand_over_kernel,
        out_shape=(
            jax.ShapeDtypeStruct(mixed.shape, mixed.dtype),
            jax.ShapeDtypeStruct(taken.shape, taken.dtype),
        ),
        in_specs=[anywhere, anywhere],
        out_specs=(anywhere, anywhere),
        scratch_shapes=[pltpu.SemaphoreType.DMA((2,))],
        compiler_params=pltpu.CompilerParams(vmem_limit_bytes=4 << 20),
    )(mixed, taken)


def on_device(
    mesh_sizes,
    candidate_embeddings,
    incoming_rms_scaling,
    probe_projector,
    address_projector,
    content_projector,
    sigmoid_mask_matrix,
    forgetting_projector,
    strength_projector_matrix,
    channel_forgetting_rates,
    forgetting_offset,
    extra_forgetting,
    outgoing_rms_scaling,
    final_projector,
    memory_matrix,
    earlier_addresses,
    earlier_contents,
    earlier_strengths,
    earlier_forgetting,
    admitted_counts,
):
    def by_lane(values):
        return values.transpose(1, 2, 0)

    mixed, taken = layer(
        mesh_sizes,
        (
            candidate_embeddings,
            incoming_rms_scaling[None, :],
            probe_projector,
            address_projector,
            content_projector,
            sigmoid_mask_matrix,
            forgetting_projector.T,
            strength_projector_matrix.T,
            channel_forgetting_rates[None, :],
            forgetting_offset[None, :],
            by_lane(extra_forgetting),
            outgoing_rms_scaling[None, :],
            final_projector,
            memory_matrix,
            earlier_addresses.reshape(-1, DK),
            earlier_contents.reshape(-1, DK),
            by_lane(earlier_strengths),
            by_lane(earlier_forgetting),
            admitted_counts[None, :],
        ),
    )
    return handed_over(mixed, taken)


def solution(mesh):
    in_specs = (
        P(("grp", "kv"), "tp"),
        P(),
        P("kv", "tp"),
        P("kv", "tp"),
        P("kv", "tp"),
        P("kv", "tp"),
        P(),
        P(),
        P("tp"),
        P("tp"),
        P(("grp", "kv"), None, "tp"),
        P(),
        P("tp", "kv"),
        P(("grp", "kv"), "tp", None, None),
        P(("grp", "kv"), None, "tp", None),
        P(("grp", "kv"), None, "tp", None),
        P(("grp", "kv"), None, "tp"),
        P(("grp", "kv"), None, "tp"),
        P(("grp", "kv")),
    )
    out_specs = (P(("grp", "kv"), "tp"), P(("grp", "kv"), "tp", None, None))
    sizes = (mesh.shape["kv"], mesh.shape["tp"])
    return jax.shard_map(
        functools.partial(on_device, sizes),
        mesh=mesh,
        in_specs=in_specs,
        out_specs=out_specs,
        check_vma=False,
    )
```

time: 132 us -> 111 us (0.84)
  Pallas kernels: 124 us -> 110 us
  local copies, waits for them, and re-layouts: 4.77 us -> 0 us
  other arithmetic: 2.09 us -> 0 us
    pallas_call x2, Pallas kernels: 124 us -> 110 us  [the longest x1 107 us: layer(): pl.pallas_call(functools.partial(mix_kernel, n_z, n_x), out_shape=(jax.Sh...]
    unnamed x8 -> x0, local copies, waits for them, and re-layouts: 2.38 us -> none
    reshape x1 -> x0, local copies, waits for them, and re-layouts: 1.63 us -> none  [on_device(): earlier_contents.reshape(rows, heads * DK)]
where the time goes in v2:
time: 111 us; the launch traced here: 110 us
  Pallas kernels  110 us (99%)
    pallas_call x1, Pallas kernels, layer(): pl.pallas_call(functools.partial(mix_kernel, n_z, n_x), out_shape=(jax.Sh...  107 us
    pallas_call x1, Pallas kernels, handed_over(): pl.pallas_call(hand_over_kernel, out_shape=(jax.ShapeDtypeStruct(mixed.sh...  2.77 us

profile of v2, /device:TPU:36, one launch (start us, length us, event | category | flops | bytes accessed | tf_op | source)
XLA Modules:
  0.0 110.5 jit_solution(17960891756422273878)
XLA Ops:
  0.6 107.1 %shard_map.194 = (bf16[192,512]{1,0:T(8,128)(2,1)S(1)}, f32[48,2,128,128]{3,2,1,0:T(8,128)S(1)}) custom-call(bf16[192,512]{1,0:T(8,128)(2,1)} %cand_ref.1, f32[1,4096]{1,0:T(1,128)} %bitcast.16, bf16[256,256]{1,0:T(8,128)(2,1)} %wq_ref.1, bf16[256,256]{1,0:T(8,128)(2,1)} %wk_ref.1, bf16[256,256]{1,0:T(8,128)(2,1)} %wv_ref.1, bf16[256,256]{1,0:T(8,128)(2,1)} %wg_ref.1, ...), custom_call_target="tpu_custom_call" | custom-call | flops 1610612736 | bytes 16777216 | tf_op jit(solution)/shard_map/pallas_call | solution.py:662
  107.7 2.8 %shard_map.195 = (bf16[192,512]{1,0:T(8,128)(2,1)}, f32[48,2,128,128]{3,2,1,0:T(8,128)}) custom-call(bf16[192,512]{1,0:T(8,128)(2,1)S(1)} %get-tuple-element.4.mixed_ref, f32[48,2,128,128]{3,2,1,0:T(8,128)S(1)} %get-tuple-element.5.taken_ref), custom_call_target="tpu_custom_call" | custom-call | tf_op jit(solution)/shard_map/pallas_call | solution.py:738

commit v3 on v2

--- a/solution.py
+++ b/solution.py
@@ -108,6 +108,7 @@
     n_buf,
     w_buf,
     f_buf,
+    t_low,
     acc,
     c_send,
     c_buf,
@@ -162,6 +163,11 @@
     x_dev = [{"tp": ((x + d) % n_x) * 2 + core} for d in range(n_x)]
     sib_dev = {"tp": x * 2 + 1 - core}
 
+    barrier = pltpu.get_barrier_semaphore()
+    peers = (z_dev[0], z_dev[1], y_dev, sib_dev, *x_dev[1:])
+    for dev in peers:
+        pl.semaphore_signal(barrier, inc=1, device_id=dev, device_id_type=MESH)
+
     def send(src, dst, s_sem, r_sem, dev):
         return pltpu.make_async_remote_copy(
             src_ref=src,
@@ -216,10 +222,6 @@
     for c in small_loads:
         c.start()
 
-    barrier = pltpu.get_barrier_semaphore()
-    peers = (z_dev[0], z_dev[1], y_dev, sib_dev, *x_dev[1:])
-    for dev in peers:
-        pl.semaphore_signal(barrier, inc=1, device_id=dev, device_id_type=MESH)
     pl.semaphore_wait(barrier, len(peers))
 
     def ring_copy(buf, subs, s_sems, r_sems, way, s, sub):
@@ -277,13 +279,12 @@
                 if s < half and goes(W_SUB, way, s + 1, sub):
                     w_copy(way, s + 1, sub).start()
 
-    def f_step(s):
-        for sub in range(F_SUB):
-            for way in range(2):
-                if goes(F_SUB, way, s, sub):
-                    f_copy(way, s, sub).wait_recv()
-                    if s < half and goes(F_SUB, way, s + 1, sub):
-                        f_copy(way, s + 1, sub).start()
+    def f_event(s, sub):
+        for way in range(2):
+            if goes(F_SUB, way, s, sub):
+                f_copy(way, s, sub).wait_recv()
+                if s < half and goes(F_SUB, way, s + 1, sub):
+                    f_copy(way, s + 1, sub).start()
 
     span = P_SIZE * heads
     old_rows = old_keys_ref.shape[0]
@@ -351,7 +352,9 @@
                 for h in range(heads):
                     scale = kept[s * span + h : s * span + h + 1, :]
                     lanes = slice((s * heads + h) * DK, (s * heads + h + 1) * DK)
-                    t_buf[i * oper + s, h] = scale * t_buf[i * oper + s, h] + added[:, lanes]
+                    fresh = scale * t_buf[i * oper + s, h] + added[:, lanes]
+                    t_buf[i * oper + s, h] = fresh
+                    t_low[i * oper + s, h] = fresh.astype(BF)
 
     strip = 16
     strips = 2 * rows // strip
@@ -429,6 +432,11 @@
         for sub in range(F_SUB):
             for way in range(2):
                 f_copy(way, 1, sub).start()
+
+    def run(jobs, subs, s, sub):
+        for place in range(sub * 4 // subs, (sub + 1) * 4 // subs):
+            for work in jobs.get((s, place), []):
+                work()
 
     plan = {
         (1, 1): [a_first],
@@ -465,9 +473,9 @@
     for s in range(1, half):
         for sub in range(W_SUB):
             w_event(s, sub)
-            for work in plan.get((s, sub), []):
-                work()
-    f_step(1)
+            run(plan, W_SUB, s, sub)
+    for sub in range(F_SUB):
+        f_event(1, sub)
     dot_steps(half - 1, half)
     for sub in range(W_SUB):
         w_event(half, sub)
@@ -483,59 +491,54 @@
     for m in range(2):
         c_buf[side, m] = acc[pl.ds(0, rows), m * width : (m + 1) * width].astype(BF)
 
-    f_step(2)
-    f_step(3)
-    for c in c_copies:
-        c.wait_recv()
-
-    for h in range(heads):
-        cols = slice(h * DK, (h + 1) * DK)
-        qn_buf[h] = unit_norm(c_buf[0, 0, :, cols].astype(F32)) * DK ** (-0.5)
-        kn_buf[h] = unit_norm(c_buf[0, 1, :, cols].astype(F32))
+    def units():
+        for c in c_copies:
+            c.wait_recv()
+        for h in range(heads):
+            cols = slice(h * DK, (h + 1) * DK)
+            qn_buf[h] = unit_norm(c_buf[0, 0, :, cols].astype(F32)) * DK ** (-0.5)
+            kn_buf[h] = unit_norm(c_buf[0, 1, :, cols].astype(F32))
 
     blk = 16
     per = blk // P_SIZE
     group = (lax.broadcasted_iota(jnp.int32, (2 * blk, DK), 0) % blk) // P_SIZE
 
     def recall(lo, hi):
-        @pl.loop(lo, hi)
-        def _(i):
-            at = pl.ds(pl.multiple_of(i * blk, blk), blk)
+        for i in range(lo, hi):
+            at = pl.ds(i * blk, blk)
             for h in range(heads):
                 both = jnp.concatenate([kn_buf[h, at, :], qn_buf[h, at, :]], axis=0).astype(BF)
                 picked = jnp.zeros((2 * blk, DK), F32)
                 for s in range(per):
-                    got = mm(both, t_buf[i * per + s, h])
+                    got = mm(both, t_low[i * per + s, h])
                     picked = jnp.where(group == s, got, picked)
                 kt_buf[h, at, :] = picked[:blk]
                 qt_buf[h, at, :] = picked[blk:]
 
-    blocks = rows // blk
-    recall(0, blocks // 2)
-    f_step(4)
-    recall(blocks // 2, blocks)
-
     masks = group_masks(rows, 1)
 
-    def attend(h):
-        cols = slice(h * DK, (h + 1) * DK)
-        summed, _, between = decay_terms(scal_buf[h], masks)
-        beta = scal_buf[heads + h]
-        keys = kn_buf[h]
-        fade = jnp.exp(summed)
-        wanted = beta * (c_buf[1, 0, :, cols].astype(F32) - fade * kt_buf[h])
-        fixes = corrections(keys, wanted, beta, between, masks)
-        pairs = between * mm_t(qn_buf[h], keys)
-        seen = fade * qt_buf[h] + mm(pairs, fixes)
-        gate = c_buf[1, 1, :, cols].astype(F32)
-        level = lax.rsqrt(jnp.mean(seen * seen, axis=1, keepdims=True) + epsilon)
-        flat[:, cols] = (
-            seen * level * out_gain_ref[...] * (gate * jax.nn.sigmoid(gate))
-        ).astype(BF)
-
-    for h in range(heads):
-        attend(h)
-    f_step(5)
+    def attend():
+        both = range(heads)
+        cols = [slice(h * DK, (h + 1) * DK) for h in both]
+        terms = [decay_terms(scal_buf[h], masks) for h in both]
+        fade = [jnp.exp(terms[h][0]) for h in both]
+        beta = [scal_buf[heads + h] for h in both]
+        like = [mm_t(kn_buf[h], kn_buf[h]) for h in both]
+        pairs = [terms[h][2] * mm_t(qn_buf[h], kn_buf[h]) for h in both]
+        lower = [jnp.where(masks[3], beta[h] * terms[h][2] * like[h], 0.0) for h in both]
+        wanted = [
+            beta[h] * (c_buf[1, 0, :, cols[h]].astype(F32) - fade[h] * kt_buf[h]) for h in both
+        ]
+        once = [mm(lower[h], wanted[h]) for h in both]
+        even = [wanted[h] + mm(lower[h], once[h]) for h in both]
+        fixes = [even[h] - mm(lower[h], even[h]) for h in both]
+        seen = [fade[h] * qt_buf[h] + mm(pairs[h], fixes[h]) for h in both]
+        for h in both:
+            gate = c_buf[1, 1, :, cols[h]].astype(F32)
+            level = lax.rsqrt(jnp.mean(seen[h] * seen[h], axis=1, keepdims=True) + epsilon)
+            flat[:, cols[h]] = (
+                seen[h] * level * out_gain_ref[...] * (gate * jax.nn.sigmoid(gate))
+            ).astype(BF)
 
     def slot_of(owner):
         return (owner // 4) * 2 + owner % 2
@@ -586,30 +589,27 @@
                 x_send[slot] = (p_buf[slot] + r_buf[slot].astype(F32)).astype(BF)
                 rx_copy(slot, dest).start()
 
-    product(me)
-
-    @pl.loop(1, 5)
-    def _(s):
-        product((me + n_z - s) % n_z)
-        product((me + s) % n_z)
-        passed_on((me + n_z - s + 1) % n_z)
-
-        @pl.when(s > 1)
-        def _():
-            passed_on((me + s - 1) % n_z)
-
-    for s in range(5, half):
-        if s > 5:
-            f_step(s)
-        product((me + n_z - s) % n_z)
-        product((me + s) % n_z)
-        passed_on((me + n_z - s + 1) % n_z)
-        passed_on((me + s - 1) % n_z)
-    f_step(half)
-    product((me + half) % n_z)
-    passed_on((me + half + 1) % n_z)
-    passed_on((me + half - 1) % n_z)
-    passed_on((me + half) % n_z)
+    def at(offset):
+        return (me + n_z + offset) % n_z
+
+    later = [functools.partial(recall, i, i + 4) for i in range(0, rows // blk, 4)]
+    late_plan = {(3, 0): [units], (3, 1): later[:1], (3, 2): later[1:2], (3, 3): later[2:]}
+    late_plan[4, 0] = [attend]
+    order = [0] + [way * d for d in range(1, half) for way in (-1, 1)]
+    spots = [(4, 1), (4, 2), (4, 3)]
+    spots += [(s, sub) for s in (half - 3, half - 2) for sub in range(4)]
+    spots += [(half - 1, 0), (half - 1, 1), (half, 0), (half, 1)]
+    for i, spot in enumerate(spots):
+        late_plan[spot] = [functools.partial(product, at(order[i]))]
+    for i, spot in enumerate(spots[2:-2] + [(half - 1, 2), (half - 1, 3), (half, 2)]):
+        late_plan.setdefault(spot, []).append(functools.partial(passed_on, at(order[i])))
+    for s in range(2, half + 1):
+        for sub in range(F_SUB):
+            f_event(s, sub)
+            run(late_plan, F_SUB, s, sub)
+    product(at(half))
+    passed_on(at(order[-1]))
+    passed_on(at(half))
 
     for d in range(1, n_x):
         for i in range(2):
@@ -673,6 +673,7 @@
             pltpu.VMEM((2 * rows, features), BF),
             pltpu.VMEM((n_z, depth, 2 * width), BF),
             pltpu.VMEM((n_z, width, depth), BF),
+            pltpu.VMEM(state.shape, BF),
             pltpu.VMEM((2 * rows, 2 * width), F32),
             pltpu.VMEM((2, rows, width), BF),
             pltpu.VMEM((2, 2, rows, width), BF),

time: 111 us -> 107 us (0.964)
  Pallas kernels: 110 us -> 107 us
    pallas_call x1, Pallas kernels: 107 us -> 104 us  [layer(): pl.pallas_call(functools.partial(mix_kernel, n_z, n_x), out_shape=(jax.Sh...]
where the time goes in v3:
time: 107 us
  Pallas kernels  107 us (100%)
    pallas_call x1, Pallas kernels, layer(): pl.pallas_call(functools.partial(mix_kernel, n_z, n_x), out_shape=(jax.Sh...  104 us
    pallas_call x1, Pallas kernels, handed_over(): pl.pallas_call(hand_over_kernel, out_shape=(jax.ShapeDtypeStruct(mixed.sh...  2.77 us

profile of v3, /device:TPU:36, one launch (start us, length us, event | category | flops | bytes accessed | tf_op | source)
XLA Modules:
  0.0 107.3 jit_solution(6051580988817220158)
XLA Ops:
  0.6 103.9 %shard_map.194 = (bf16[192,512]{1,0:T(8,128)(2,1)S(1)}, f32[48,2,128,128]{3,2,1,0:T(8,128)S(1)}) custom-call(bf16[192,512]{1,0:T(8,128)(2,1)} %cand_ref.1, f32[1,4096]{1,0:T(1,128)} %bitcast.16, bf16[256,256]{1,0:T(8,128)(2,1)} %wq_ref.1, bf16[256,256]{1,0:T(8,128)(2,1)} %wk_ref.1, bf16[256,256]{1,0:T(8,128)(2,1)} %wv_ref.1, bf16[256,256]{1,0:T(8,128)(2,1)} %wg_ref.1, ...), custom_call_target="tpu_custom_call" | custom-call | flops 1610612736 | bytes 16777216 | tf_op jit(solution)/shard_map/pallas_call | solution.py:662
  104.5 2.8 %shard_map.195 = (bf16[192,512]{1,0:T(8,128)(2,1)}, f32[48,2,128,128]{3,2,1,0:T(8,128)}) custom-call(bf16[192,512]{1,0:T(8,128)(2,1)S(1)} %get-tuple-element.4.mixed_ref, f32[48,2,128,128]{3,2,1,0:T(8,128)S(1)} %get-tuple-element.5.taken_ref), custom_call_target="tpu_custom_call" | custom-call | tf_op jit(solution)/shard_map/pallas_call | solution.py:739

commit v4 on v3

--- a/solution.py
+++ b/solution.py
@@ -11,6 +11,7 @@
 P_SIZE = 4
 W_SUB = 4
 F_SUB = 4
+FIRST_SUB = 2
 VMEM_BYTES = 67043328
 
 epsilon = 1e-06
@@ -233,17 +234,17 @@
         )
 
     def w_copy(way, s, sub):
-        return ring_copy(w_buf, W_SUB, w_send, w_recv, way, s, sub)
+        return ring_copy(w_buf, FIRST_SUB if s == 1 else W_SUB, w_send, w_recv, way, s, sub)
 
     def f_copy(way, s, sub):
-        return ring_copy(f_buf, F_SUB, f_send, f_recv, way, s, sub)
+        return ring_copy(f_buf, FIRST_SUB if s == 1 else F_SUB, f_send, f_recv, way, s, sub)
 
     def goes(subs, way, s, sub):
         return s < half or (sub * 2) // subs == way
 
     w_load(wq_ref, 0).wait()
     w_load(wk_ref, 1).wait()
-    for sub in range(W_SUB):
+    for sub in range(FIRST_SUB):
         for way in range(2):
             w_copy(way, 1, sub).start()
     cand_load.wait()
@@ -273,18 +274,26 @@
     a_sib(0, 0).start()
 
     def w_event(s, sub):
+        span = W_SUB // FIRST_SUB if s == 1 else 1
+        if sub % span:
+            return
         for way in range(2):
             if goes(W_SUB, way, s, sub):
-                w_copy(way, s, sub).wait_recv()
-                if s < half and goes(W_SUB, way, s + 1, sub):
-                    w_copy(way, s + 1, sub).start()
+                w_copy(way, s, sub // span).wait_recv()
+                for piece in range(sub, sub + span):
+                    if s < half and goes(W_SUB, way, s + 1, piece):
+                        w_copy(way, s + 1, piece).start()
 
     def f_event(s, sub):
+        span = F_SUB // FIRST_SUB if s == 1 else 1
+        if sub % span:
+            return
         for way in range(2):
             if goes(F_SUB, way, s, sub):
-                f_copy(way, s, sub).wait_recv()
-                if s < half and goes(F_SUB, way, s + 1, sub):
-                    f_copy(way, s + 1, sub).start()
+                f_copy(way, s, sub // span).wait_recv()
+                for piece in range(sub, sub + span):
+                    if s < half and goes(F_SUB, way, s + 1, piece):
+                        f_copy(way, s + 1, piece).start()
 
     span = P_SIZE * heads
     old_rows = old_keys_ref.shape[0]
@@ -429,7 +438,7 @@
 
     def f_begin():
         f_load.wait()
-        for sub in range(F_SUB):
+        for sub in range(FIRST_SUB):
             for way in range(2):
                 f_copy(way, 1, sub).start()
 
@@ -630,10 +639,10 @@
             a_sib(part, d).wait_send()
     for s in range(1, half + 1):
         for way in range(2):
-            for sub in range(W_SUB):
+            for sub in range(FIRST_SUB if s == 1 else W_SUB):
                 if goes(W_SUB, way, s, sub):
                     w_copy(way, s, sub).wait_send()
-            for sub in range(F_SUB):
+            for sub in range(FIRST_SUB if s == 1 else F_SUB):
                 if goes(F_SUB, way, s, sub):
                     f_copy(way, s, sub).wait_send()
     for c in c_copies:

time: 107 us -> 108 us (level)
  no operation moved by 1% of the time
where the time goes in v4:
time: 108 us
  Pallas kernels  108 us (100%)
    pallas_call x1, Pallas kernels, layer(): pl.pallas_call(functools.partial(mix_kernel, n_z, n_x), out_shape=(jax.Sh...  105 us
    pallas_call x1, Pallas kernels, handed_over(): pl.pallas_call(hand_over_kernel, out_shape=(jax.ShapeDtypeStruct(mixed.sh...  2.77 us

profile of v4, /device:TPU:36, one launch (start us, length us, event | category | flops | bytes accessed | tf_op | source)
XLA Modules:
  0.0 108.3 jit_solution(9252616001674794452)
XLA Ops:
  0.6 104.9 %shard_map.194 = (bf16[192,512]{1,0:T(8,128)(2,1)S(1)}, f32[48,2,128,128]{3,2,1,0:T(8,128)S(1)}) custom-call(bf16[192,512]{1,0:T(8,128)(2,1)} %cand_ref.1, f32[1,4096]{1,0:T(1,128)} %bitcast.16, bf16[256,256]{1,0:T(8,128)(2,1)} %wq_ref.1, bf16[256,256]{1,0:T(8,128)(2,1)} %wk_ref.1, bf16[256,256]{1,0:T(8,128)(2,1)} %wv_ref.1, bf16[256,256]{1,0:T(8,128)(2,1)} %wg_ref.1, ...), custom_call_target="tpu_custom_call" | custom-call | flops 1610612736 | bytes 16777216 | tf_op jit(solution)/shard_map/pallas_call | solution.py:671
  105.5 2.8 %shard_map.195 = (bf16[192,512]{1,0:T(8,128)(2,1)}, f32[48,2,128,128]{3,2,1,0:T(8,128)}) custom-call(bf16[192,512]{1,0:T(8,128)(2,1)S(1)} %get-tuple-element.4.mixed_ref, f32[48,2,128,128]{3,2,1,0:T(8,128)S(1)} %get-tuple-element.5.taken_ref), custom_call_target="tpu_custom_call" | custom-call | tf_op jit(solution)/shard_map/pallas_call | solution.py:748
